TPU v7x, 512 devices: a whole 4x4x16 slice. The times are simulated.
512 devices in a mesh: ep: 32 (over z, core), tp: 16 (over y, x).
Axes of the slice: x: 4, y: 4, z: 16, core: 2. Of those that a mesh axis runs over, the one named last changes fastest.
Arguments:
- queries: bfloat16 [8192, 4096], P('ep', 'tp'), may hold values from -6 to 6
- keys: bfloat16 [8192, 1024], P('ep', 'tp'), may hold values from -6 to 6
- values: bfloat16 [8192, 1024], P('ep', 'tp'), may hold values from -6 to 6
- query_gain: float32 [64], replicated, may hold values from 1 to 11
- key_gain: float32 [64], replicated, may hold values from 1 to 11
- moe_rows: bfloat16 [8192, 4096], P('ep', 'tp'), may hold values from -14 to 14
- route_ids: int32 [8192, 2], P('ep'), may hold values from 0 to 31, all different within a row; in each aligned block of 256 rows (0 to 255, 256 to 511, ...) at most 24 rows name the same one
- group_weight: float32 [8192], P('ep'), may hold values from 0.2 to 1
- expert_weight: float32 [8192, 2], P('ep'), may hold values from 0.05 to 1
- expert_gate: bfloat16 [32, 4096, 2048], P('ep', None, 'tp'), may hold values from -0.09375 to 0.09375
- expert_up: bfloat16 [32, 4096, 2048], P('ep', None, 'tp'), may hold values from -0.09375 to 0.09375
- expert_down: bfloat16 [32, 2048, 4096], P('ep', None, 'tp'), may hold values from -0.125 to 0.125
Outputs:
- attended: bfloat16 [8192, 4096], P('ep', 'tp')
- moe_out: bfloat16 [8192, 4096], P('ep', 'tp')
Inputs may be any that keep to these rules, and one draw needn't show every extreme that they name: `route_ids`: each row names 2 different experts. Among the rows of one device no expert is named by more than 24 rows, and in every draw some expert is named by exactly 24 of them.
All inputs are finite; a program needn't handle non-finite values.
Results may differ from a plain program's by a relative error of at most 0.0055.
The roundings to bfloat16 on the way count: a program that leaves them out, or rounds other values in their place, can miss the bound.
Values may be sent and summed in bfloat16 or wider, within the bound.
No kernel may reach another device: no remote copies, remote signals or barrier semaphores. Data moves between devices by JAX's collectives and lax.ppermute only.
A program may use at most 128 MiB of HBM per device.

v0:
```python
import functools

import jax
import jax.numpy as jnp
from jax import lax
from jax.experimental import pallas as pl
from jax.experimental.pallas import tpu as pltpu
from jax.sharding import Mesh
from jax.sharding import PartitionSpec as P

D = 4096
HEAD_DIM = 64
GRID_W = 64
TOK = 256
EXPERTS = 32
CAP = 24
SLOTS = EXPERTS * CAP
HALF = SLOTS // 2
PAIRS = HEAD_DIM // 4
EXTRA = 8
EP = ("z", "c")
TP = ("y", "x")
CX = ("c", "x")
CY = ("c", "y")
BF = jnp.bfloat16
F32 = jnp.float32


def iota(shape, dim):
    return lax.broadcasted_iota(jnp.int32, shape, dim)


def mm(a, b):
    return jnp.dot(a, b, preferred_element_type=F32)


def column(row):
    n = row.shape[1]
    eye = iota((n, n), 0) == iota((n, n), 1)
    return jnp.sum(jnp.where(eye, jnp.broadcast_to(row, (n, n)), 0.0), axis=1, keepdims=True)


def slots_of(ids):
    e = iota((EXPERTS, TOK), 0)
    hits = [e == ids[k : k + 1] for k in range(2)]
    member = jnp.where(hits[0] | hits[1], 1.0, 0.0).astype(BF)
    before = jnp.where(iota((TOK, TOK), 0) < iota((TOK, TOK), 1), 1.0, 0.0).astype(BF)
    rank = mm(member, before)
    return [
        ids[k : k + 1] * CAP
        + jnp.sum(jnp.where(hits[k], rank, 0.0), axis=0, keepdims=True).astype(jnp.int32)
        for k in range(2)
    ]


def route_fn(ids, rows):
    first, second = slots_of(ids)
    s = iota((SLOTS, TOK), 0)
    chosen = jnp.where((s == first) | (s == second), 1.0, 0.0).astype(BF)
    return mm(chosen, rows).astype(BF)


def combine_fn(ids, group_weight, expert_weight, results):
    total = expert_weight[0:1] + expert_weight[1:2]
    out = None
    for k, slot in enumerate(slots_of(ids)):
        mix = column(group_weight * expert_weight[k : k + 1] / total)
        at = column(slot.astype(F32)).astype(jnp.int32)
        chosen = jnp.where(iota((TOK, SLOTS), 1) == at, 1.0, 0.0).astype(BF)
        part = mix * mm(chosen, results)
        out = part if out is None else out + part
    return out.astype(BF)


def rotated(x, gain, table):
    mean = jnp.sum(x * x, axis=0, keepdims=True) * (1.0 / HEAD_DIM)
    scaled = x * lax.rsqrt(mean + 1e-06) * gain
    parts = []
    for axis in range(2):
        lo = 2 * PAIRS * axis
        x1, x2 = scaled[lo : lo + PAIRS], scaled[lo + PAIRS : lo + 2 * PAIRS]
        cosine = table[PAIRS * axis : PAIRS * (axis + 1)]
        sine = table[PAIRS * (axis + 2) : PAIRS * (axis + 3)]
        parts += [x1 * cosine - x2 * sine, x2 * cosine + x1 * sine]
    return jnp.concatenate(parts, axis=0)


def rope_fn(queries, keys_t, values_t, table):
    q_t = queries.astype(F32).T
    q_gain, k_gain = table[64:128], table[128:192]
    heads = []
    for h in range(4):
        turned = rotated(q_t[h * HEAD_DIM : (h + 1) * HEAD_DIM], q_gain, table) * 0.125
        heads.append(jnp.concatenate([turned, jnp.zeros_like(turned)], axis=0).T.astype(BF))
    k = rotated(keys_t.astype(F32), k_gain, table)
    kv = jnp.concatenate([k, values_t.astype(F32)], axis=0).T.astype(BF)
    return heads, kv


def gate_up_fn(get_tokens, get_weight, put):
    ones = jnp.ones((EXTRA, 256), BF)
    rows = []
    sums = []
    for c in range(2):
        blocks = [get_tokens(4 * c + x) for x in range(4)]
        square = None
        for b in blocks:
            w = b.astype(F32)
            square = w * w if square is None else square + w * w
        total = None
        for _ in range(3):
            piece = square.astype(BF)
            square = square - piece.astype(F32)
            part = lax.dot_general(ones, piece, (((1,), (1,)), ((), ())), preferred_element_type=F32)
            total = part if total is None else total + part
        sums.append(total[0:1])
        rows.append(jnp.concatenate(blocks, axis=1))
    sums = jnp.concatenate(sums, axis=1) * 0.125
    high = sums.astype(BF).astype(F32)
    low = (sums - high) * 256.0
    pieces = [v[:, 256 * i : 256 * (i + 1)] for v in (high, low) for i in range(3)]
    extra = jnp.concatenate(pieces + [jnp.zeros((2, 256), F32)], axis=0)
    for s in range(4):
        w = get_weight(s)
        for c in range(2):
            put(s, c * HALF, mm(rows[c], w) * 32.0)
        put(s, SLOTS, extra)


def hidden_fn(get, put):
    sums = get(SLOTS, EXTRA)
    for i in range(3):
        square = (sums[i : i + 1] + sums[i + 3 : i + 4] * (1.0 / 256)) * (8.0 / D)
        inv = lax.rsqrt(column(square) + 1e-06) * (1.0 / 32)
        both = get(256 * i, 256)
        gate, up = both[:, :128] * inv, both[:, 128:] * inv
        put(256 * i, (gate / (1.0 + jnp.exp(-gate)) * up).astype(BF))


def down_fn(get_hidden, get_weight, put):
    rows = [
        [jnp.concatenate([get_hidden(2 * j, c), get_hidden(2 * j + 1, c)], axis=1) for j in range(2)]
        for c in range(2)
    ]
    for s in range(4):
        w = get_weight(s)
        for c in range(2):
            put(c, s, (mm(rows[c][0], w[:256]) + mm(rows[c][1], w[256:])).astype(BF))


def reduce_fn(get):
    return [
        sum(get(4 * c + y).astype(F32) for y in range(4)).astype(BF).reshape(16, CAP, 256)
        for c in range(2)
    ]


def route_kernel(ids, rows, out):
    out[...] = route_fn(ids[...], rows[...])


def combine_kernel(ids, gw, ew, res, out):
    out[...] = combine_fn(ids[...], gw[...], ew[...], res[...])


def rope_kernel(q, k, v, table, q_first, q_second, kv_out):
    heads, kv = rope_fn(q[...], k[...], v[...], table[...])
    for h in range(2):
        q_first[h] = heads[h]
        q_second[h] = heads[2 + h]
    kv_out[...] = kv


def pack_kernel(at, gate, up, down, *outs):
    for s in range(4):
        y = lax.rem(at[0] + s, 4)
        rows = pl.ds(pl.multiple_of(y * 1024, 1024), 1024)
        outs[s][0:1024, 0:128] = gate[rows, :]
        outs[s][0:1024, 128:256] = up[rows, :]
        outs[s][1024:1536, :] = down[pl.ds(pl.multiple_of(y * 512, 512), 512), :]


def gate_up_kernel(at, tokens, w0, w1, w2, w3, out):
    weights = (w0, w1, w2, w3)

    def put(s, row, value):
        out[lax.rem(at[0] + 4 - s, 4), row : row + value.shape[0], :] = value

    gate_up_fn(lambda i: tokens[i], lambda s: weights[s][0:1024, :], put)


def hidden_kernel(parts, out):
    def put(at, value):
        for y in range(4):
            out[y, at : at + value.shape[0], :] = value

    hidden_fn(lambda at, n: parts[at : at + n, :], put)


def down_kernel(at, hidden, w0, w1, w2, w3, out):
    weights = (w0, w1, w2, w3)

    def put(c, s, value):
        out[c, lax.rem(at[0] + 4 - s, 4)] = value

    down_fn(
        lambda x, c: hidden[x, c * HALF : (c + 1) * HALF, :],
        lambda s: weights[s][1024:1536, :],
        put,
    )


def reduce_kernel(parts, out):
    for c, value in enumerate(reduce_fn(lambda i: parts[i])):
        out[:, c] = value


KEYS = 1024


def attend_kernel(q, kv, out, scores):
    blocks = [(kv, i) for i in range(kv.shape[0] // KEYS)]

    def lanes(v, op):
        parts = [v[:, 128 * i : 128 * (i + 1)] for i in range(v.shape[1] // 128)]
        return functools.reduce(op, parts)

    def score(h, j):
        ref, i = blocks[j]
        s = lax.dot_general(
            q[h], ref[i * KEYS : (i + 1) * KEYS, :], (((1,), (1,)), ((), ())), preferred_element_type=F32
        )
        scores[h, :, j * KEYS : (j + 1) * KEYS] = s
        return lanes(s, jnp.maximum)

    def weigh(h, j, top):
        ref, i = blocks[j]
        p = jnp.exp(scores[h, :, j * KEYS : (j + 1) * KEYS] - top)
        return lanes(p, jnp.add), mm(p.astype(BF), ref[i * KEYS : (i + 1) * KEYS, :])

    n = len(blocks)
    top = functools.reduce(jnp.maximum, [score(0, j) for j in range(n)])
    results = []
    for h in range(2):
        top = jnp.max(top, axis=1, keepdims=True)
        following = total = summed = None
        for j in range(n):
            if h == 0:
                m = score(1, j)
                following = m if following is None else jnp.maximum(following, m)
            t, o = weigh(h, j, top)
            total = t if total is None else total + t
            summed = o if summed is None else summed + o
        top = following
        results.append(summed / jnp.sum(total, axis=1, keepdims=True))
    first = pltpu.roll(results[0], HEAD_DIM, axis=1)
    out[...] = jnp.where(iota(first.shape, 1) < HEAD_DIM, first, results[1]).astype(BF)


def call(kernel, outs, *args, flops=0, scratch=(), vmem=20, space=pltpu.VMEM):
    def spec(a):
        return pl.BlockSpec(memory_space=pltpu.SMEM if a.dtype == jnp.int32 and a.size == 1 else space)

    return pl.pallas_call(
        kernel,
        out_shape=outs,
        in_specs=[spec(a) for a in args],
        out_specs=jax.tree.map(lambda _: pl.BlockSpec(memory_space=space), outs),
        scratch_shapes=scratch,
        cost_estimate=pl.CostEstimate(flops=flops, transcendentals=0, bytes_accessed=0),
        compiler_params=pltpu.CompilerParams(vmem_limit_bytes=vmem << 20),
    )(*args)


def array(*shape, dtype=BF):
    return jax.ShapeDtypeStruct(shape, dtype)


def shifted(blocks, axis):
    return [b if s == 0 else lax.ppermute(b, axis, [(i, (i + s) % 4) for i in range(4)]) for s, b in enumerate(blocks)]


def exchange(a, axes):
    return lax.all_to_all(a, axes, split_axis=0, concat_axis=0, tiled=True)


def rope_table(query_gain, key_gain):
    position = lax.axis_index(EP) * TOK + jnp.arange(TOK, dtype=jnp.int32)
    grid_pos = jnp.stack([position // GRID_W, position % GRID_W], axis=0).astype(F32)
    frequency = 10000.0 ** (-jnp.arange(PAIRS, dtype=F32) / PAIRS)
    angles = (grid_pos[:, None, :] * frequency[None, :, None]).reshape(2 * PAIRS, TOK)
    gains = jnp.concatenate([query_gain, key_gain])
    return jnp.concatenate(
        [jnp.cos(angles), jnp.sin(angles), jnp.broadcast_to(gains[:, None], (2 * HEAD_DIM, TOK))], axis=0
    )


def attend(q, kv):
    scratch = [pltpu.VMEM((2, TOK, kv.shape[0]), F32)]
    return call(attend_kernel, array(TOK, 128), q, kv, flops=2200 << 20, scratch=scratch, vmem=36)


def on_device(
    queries,
    keys,
    values,
    query_gain,
    key_gain,
    moe_rows,
    route_ids,
    group_weight,
    expert_weight,
    expert_gate,
    expert_up,
    expert_down,
):
    tie = lax.optimization_barrier
    ids = route_ids.T
    routed = call(route_kernel, array(SLOTS, 256), ids, moe_rows, flops=4 << 20)
    arrived = exchange(routed.reshape(16, 2 * CAP, 256), "z")
    table = rope_table(query_gain, key_gain)
    *q_heads, kv = call(
        rope_kernel,
        (array(2, TOK, 128),) * 2 + (array(TOK, 128),),
        queries,
        keys.T,
        values.T,
        table,
        flops=4 << 20,
    )
    kv = lax.all_gather(kv, EP, axis=0, tiled=True)
    at = lax.axis_index("y").astype(jnp.int32).reshape(1)
    packed = call(pack_kernel, (array(1536, 256),) * 4, at, expert_gate[0], expert_up[0], expert_down[0])
    weights = shifted(packed, "y")
    arrived, q_heads = tie((arrived, q_heads))
    sent = arrived.reshape(16, 2, CAP, 256).transpose(1, 0, 2, 3).reshape(2, 1, HALF, 256)
    tokens = exchange(jnp.broadcast_to(sent, (2, 4, HALF, 256)).reshape(8, HALF, 256), CX)
    partial = call(
        gate_up_kernel, array(4, SLOTS + EXTRA, 256, dtype=F32), at, tokens, *weights, flops=1600 << 20
    ).astype(jnp.float16)
    products = exchange(partial, "y")
    hidden = call(
        hidden_kernel, array(4, SLOTS, 128), jnp.sum(products.astype(F32), axis=0), flops=8 << 20
    )
    hidden = exchange(hidden, "x")
    results = call(
        down_kernel, array(2, 4, HALF, 256), at, hidden, *weights, flops=800 << 20
    ).reshape(8, HALF, 256)
    results, q_heads = tie((results, q_heads))
    summands = exchange(results, CY)
    attended = jnp.concatenate([attend(q, kv) for q in q_heads], axis=1)
    summands, attended = tie((summands, attended))
    reduced = call(reduce_kernel, array(16, 2, CAP, 256), summands, flops=4 << 20)
    returned = exchange(reduced.reshape(16, 2 * CAP, 256), "z")
    moe_out = call(
        combine_kernel,
        array(TOK, 256),
        ids,
        group_weight.reshape(1, TOK),
        expert_weight.T,
        returned.reshape(SLOTS, 256),
        flops=8 << 20,
    )
    return (attended, moe_out)


def solution(mesh):
    torus = Mesh(mesh.devices.reshape(16, 2, 4, 4), ("z", "c", "y", "x"))

    return jax.shard_map(
        on_device,
        mesh=torus,
        in_specs=(
            P(EP, TP),
            P(EP, TP),
            P(EP, TP),
            P(),
            P(),
            P(EP, TP),
            P(EP, None),
            P(EP),
            P(EP, None),
            P(EP, None, TP),
            P(EP, None, TP),
            P(EP, None, TP),
        ),
        out_specs=(P(EP, TP), P(EP, TP)),
        check_vma=False,
    )
```

profile of v0, /device:TPU:8, one launch (start us, length us, event | category | flops | bytes accessed | tf_op | source)
XLA Modules:
  0.0 211.7 jit_solution(15176611220340141932)
XLA Ops:
  7.2 0.9 copy-done.10
  8.8 1.2 shard_map.131
  10.0 15.2 %all-to-all-start = ((bf16[16,48,256]{2,1,0:T(8,128)(2,1)}), bf16[16,48,256]{2,1,0:T(8,128)(2,1)S(1)}, u32[]{:S(2)}, u32[]{:S(2)}) async-start(bf16[16,48,256]{2,1,0:T(8,128)(2,1)} %bitcast.2), calls=%async_computation | async-start | bytes 786432 | tf_op jit(solution)/shard_map/all_to_all | solution.py:284
  25.6 0.8 pad_maximum_fusion.1
  26.4 0.9 shard_map.132
  28.0 21.0 %all-to-all-done = bf16[16,48,256]{2,1,0:T(8,128)(2,1)S(1)} async-done(((bf16[16,48,256]{2,1,0:T(8,128)(2,1)}), bf16[16,48,256]{2,1,0:T(8,128)(2,1)S(1)}, u32[]{:S(2)}, u32[]{:S(2)}) %all-to-all-start) | async-done | bytes 393248 | tf_op jit(solution)/shard_map/all_to_all | solution.py:284
  49.0 1.2 broadcast_in_dim.8
  50.3 4.4 %all-to-all-start.1 = ((bf16[8,384,256]{2,1,0:T(8,128)(2,1)}), bf16[8,384,256]{2,1,0:T(8,128)(2,1)S(1)}, u32[]{:S(2)}, u32[]{:S(2)}) async-start(bf16[8,384,256]{2,1,0:T(8,128)(2,1)} %bitcast.35), calls=%async_computation.1 | async-start | bytes 3145728 | tf_op jit(solution)/shard_map/all_to_all | solution.py:284
  54.8 0.7 all-gather.2.cloned.1.call-update
  55.5 1.2 copy-done.7
  56.7 1.2 copy-done.8
  58.3 3.5 %collective-permute-start = (bf16[1536,256]{1,0:T(8,128)(2,1)S(1)}, bf16[1536,256]{1,0:T(8,128)(2,1)S(1)}, u32[]{:S(2)}, u32[]{:S(2)}) collective-permute-start(bf16[1536,256]{1,0:T(8,128)(2,1)S(1)} %get-tuple-element.21), channel_id=1, source_target_pairs={{0,4},{4,8},{8,12},{12,0},{1,5},{5,9},{9,13},{13,1},{2,6},{6,10},{... | collective-permute-start | bytes 2359304 | tf_op jit(solution)/shard_map/ppermute | solution.py:280
  61.8 2.8 %collective-permute-start.1 = (bf16[1536,256]{1,0:T(8,128)(2,1)S(1)}, bf16[1536,256]{1,0:T(8,128)(2,1)S(1)}, u32[]{:S(2)}, u32[]{:S(2)}) collective-permute-start(bf16[1536,256]{1,0:T(8,128)(2,1)S(1)} %get-tuple-element.22), channel_id=1, source_target_pairs={{0,8},{4,12},{8,0},{12,4},{1,9},{5,13},{9,1},{13,5},{2,10},{6,14},... | collective-permute-start | bytes 2359304 | tf_op jit(solution)/shard_map/ppermute | solution.py:280
  64.7 4.3 %collective-permute-start.2 = (bf16[1536,256]{1,0:T(8,128)(2,1)S(1)}, bf16[1536,256]{1,0:T(8,128)(2,1)S(1)}, u32[]{:S(2)}, u32[]{:S(2)}) collective-permute-start(bf16[1536,256]{1,0:T(8,128)(2,1)S(1)} %get-tuple-element.23), channel_id=1, source_target_pairs={{0,12},{4,0},{8,4},{12,8},{1,13},{5,1},{9,5},{13,9},{2,14},{6,2},{... | collective-permute-start | bytes 2359304 | tf_op jit(solution)/shard_map/ppermute | solution.py:280
  69.0 11.6 %collective-permute-done.w1 = bf16[1536,256]{1,0:T(8,128)(2,1)S(1)} collective-permute-done((bf16[1536,256]{1,0:T(8,128)(2,1)S(1)}, bf16[1536,256]{1,0:T(8,128)(2,1)S(1)}, u32[]{:S(2)}, u32[]{:S(2)}) %collective-permute-start) | collective-permute-done | bytes 786464 | tf_op jit(solution)/shard_map/ppermute | solution.py:280
  80.6 5.0 %collective-permute-done.1.w2 = bf16[1536,256]{1,0:T(8,128)(2,1)S(1)} collective-permute-done((bf16[1536,256]{1,0:T(8,128)(2,1)S(1)}, bf16[1536,256]{1,0:T(8,128)(2,1)S(1)}, u32[]{:S(2)}, u32[]{:S(2)}) %collective-permute-start.1) | collective-permute-done | bytes 786464 | tf_op jit(solution)/shard_map/ppermute | solution.py:280
  85.7 0.9 copy-done
  86.6 15.2 %collective-permute-done.2.w3 = bf16[1536,256]{1,0:T(8,128)(2,1)S(1)} collective-permute-done((bf16[1536,256]{1,0:T(8,128)(2,1)S(1)}, bf16[1536,256]{1,0:T(8,128)(2,1)S(1)}, u32[]{:S(2)}, u32[]{:S(2)}) %collective-permute-start.2) | collective-permute-done | bytes 786464 | tf_op jit(solution)/shard_map/ppermute | solution.py:280
  101.7 0.9 copy-done.3
  102.7 1.1 copy-done.1
  103.8 1.1 copy-done.4
  104.9 2.3 %shard_map.134 = f32[4,776,256]{2,1,0:T(8,128)S(1)} custom-call(s32[1]{0:T(128)} %bitcast.at, bf16[8,384,256]{2,1,0:T(8,128)(2,1)S(1)} %all-to-all-done.1.tokens, bf16[1536,256]{1,0:T(8,128)(2,1)S(1)} %get-tuple-element.20.w0, bf16[1536,256]{1,0:T(8,128)(2,1)S(1)} %collective-permute-done.w1, bf16[1536,256]{1,0:T(8,128)(2,1)S(1)} %copy-done.1, ...), custom_call_target="tpu_custom_call" | custom-call | flops 1677721600 | tf_op jit(solution)/shard_map/pallas_call | solution.py:264
  107.5 22.9 %all_to_all.30 = f16[4,776,256]{2,1,0:T(8,128)(2,1)S(1)} all-to-all(f16[4,776,256]{2,1,0:T(8,128)(2,1)S(1)} %convert_element_type.14), channel_id=1, replica_groups=mesh['z'=16,'c'=2,'y'=4,'x'=4] {'y'}, dimensions={0} | all-to-all | bytes 3178496 | tf_op jit(solution)/shard_map/all_to_all | solution.py:284
  130.9 15.1 %all_to_all.31.hidden = bf16[4,768,128]{2,1,0:T(8,128)(2,1)S(1)} all-to-all(bf16[4,768,128]{2,1,0:T(8,128)(2,1)S(1)} %shard_map.135), channel_id=1, replica_groups=mesh['z'=16,'c'=2,'y'=4,'x'=4] {'x'}, dimensions={0} | all-to-all | bytes 1572864 | tf_op jit(solution)/shard_map/all_to_all | solution.py:284
  146.0 2.1 %shard_map.136 = bf16[2,4,384,256]{3,2,1,0:T(8,128)(2,1)} custom-call(s32[1]{0:T(128)} %bitcast.at, bf16[4,768,128]{2,1,0:T(8,128)(2,1)S(1)} %all_to_all.31.hidden, bf16[1536,256]{1,0:T(8,128)(2,1)S(1)} %get-tuple-element.20.w0, bf16[1536,256]{1,0:T(8,128)(2,1)S(1)} %collective-permute-done.w1, bf16[1536,256]{1,0:T(8,128)(2,1)S(1)} %copy-done.2, ...), custom_call_target="tpu_custom_call" | custom-call | flops 838860800 | tf_op jit(solution)/shard_map/pallas_call | solution.py:264
  148.1 5.1 %all-to-all-start.4 = ((bf16[8,384,256]{2,1,0:T(8,128)(2,1)}), bf16[8,384,256]{2,1,0:T(8,128)(2,1)S(1)}, u32[]{:S(2)}, u32[]{:S(2)}) async-start(bf16[8,384,256]{2,1,0:T(8,128)(2,1)} %bitcast.13), calls=%async_computation.4 | async-start | bytes 3145728 | tf_op jit(solution)/shard_map/all_to_all | solution.py:284
  153.2 1.6 copy-done.17
  154.8 5.9 %shard_map.137 = bf16[256,128]{1,0:T(8,128)(2,1)S(1)} custom-call(bf16[2,256,128]{2,1,0:T(8,128)(2,1)S(1)} %copy-done.19, bf16[8192,128]{1,0:T(8,128)(2,1)S(1)} %copy-done.17), custom_call_target="tpu_custom_call" | custom-call | flops 2306867200 | tf_op jit(solution)/shard_map/pallas_call | solution.py:264
  160.7 5.9 %shard_map.138 = bf16[256,128]{1,0:T(8,128)(2,1)S(1)} custom-call(bf16[2,256,128]{2,1,0:T(8,128)(2,1)S(1)} %get-tuple-element.29.q, bf16[8192,128]{1,0:T(8,128)(2,1)S(1)} %copy-done.17), custom_call_target="tpu_custom_call" | custom-call | flops 2306867200 | tf_op jit(solution)/shard_map/pallas_call | solution.py:264
  167.3 5.5 %all-to-all-done.4.parts = bf16[8,384,256]{2,1,0:T(8,128)(2,1)S(1)} async-done(((bf16[8,384,256]{2,1,0:T(8,128)(2,1)}), bf16[8,384,256]{2,1,0:T(8,128)(2,1)S(1)}, u32[]{:S(2)}, u32[]{:S(2)}) %all-to-all-start.4) | async-done | bytes 1572896 | tf_op jit(solution)/shard_map/all_to_all | solution.py:284
  173.0 30.6 %all_to_all.32 = bf16[16,48,256]{2,1,0:T(8,128)(2,1)S(1)} all-to-all(bf16[16,48,256]{2,1,0:T(8,128)(2,1)S(1)} %bitcast.25), channel_id=1, replica_groups=mesh['z'=16,'c'=2,'y'=4,'x'=4] {'z'}, dimensions={0} | all-to-all | bytes 786432 | tf_op jit(solution)/shard_map/all_to_all | solution.py:284
  203.6 1.3 shard_map.140
  (49 shorter events, 3.9 us)
Async XLA Ops:
  7.2 19.2 %copy-start.9 = (bf16[256,256]{1,0:T(8,128)(2,1)S(1)}, bf16[256,256]{1,0:T(8,128)(2,1)}, u32[]{:S(2)}) copy-start(bf16[256,256]{1,0:T(8,128)(2,1)} %q.1) | copy-start | bytes 393220
  7.2 0.9 copy-start.10
  8.1 0.7 copy-start.13
  8.8 17.6 %copy-start.11 = (bf16[256,64]{0,1:T(8,128)(2,1)S(1)}, bf16[256,64]{0,1:T(8,128)(2,1)}, u32[]{:S(2)}) copy-start(bf16[256,64]{0,1:T(8,128)(2,1)} %param.13) | copy-start | bytes 98308
  8.8 17.6 %copy-start.12 = (bf16[256,64]{0,1:T(8,128)(2,1)S(1)}, bf16[256,64]{0,1:T(8,128)(2,1)}, u32[]{:S(2)}) copy-start(bf16[256,64]{0,1:T(8,128)(2,1)} %param.14) | copy-start | bytes 98308
  10.0 39.0 %all-to-all-start = ((bf16[16,48,256]{2,1,0:T(8,128)(2,1)}), bf16[16,48,256]{2,1,0:T(8,128)(2,1)S(1)}, u32[]{:S(2)}, u32[]{:S(2)}) async-start(bf16[16,48,256]{2,1,0:T(8,128)(2,1)} %bitcast.2), calls=%async_computation | async-start | bytes 786432 | tf_op jit(solution)/shard_map/all_to_all | solution.py:284
  27.4 0.7 copy-start.18
  50.3 5.2 %copy-start.6 = (bf16[1,4096,128]{2,1,0:T(8,128)(2,1)S(1)}, bf16[1,4096,128]{2,1,0:T(8,128)(2,1)}, u32[]{:S(2)}) copy-start(bf16[1,4096,128]{2,1,0:T(8,128)(2,1)} %param.21) | copy-start | bytes 3145732
  50.3 52.4 %all-to-all-start.1 = ((bf16[8,384,256]{2,1,0:T(8,128)(2,1)}), bf16[8,384,256]{2,1,0:T(8,128)(2,1)S(1)}, u32[]{:S(2)}, u32[]{:S(2)}) async-start(bf16[8,384,256]{2,1,0:T(8,128)(2,1)} %bitcast.35), calls=%async_computation.1 | async-start | bytes 3145728 | tf_op jit(solution)/shard_map/all_to_all | solution.py:284
  54.7 98.5 %all-gather.2.cloned.1.call-start = ((), (), s32[]{:S(2)}) async-start(), calls=%async_computation.6 | async-start | bytes 2162688 | tf_op jit(solution)/shard_map/all_gather | solution.py:331
  55.5 1.2 copy-start.7
  56.7 1.2 copy-start.8
  58.3 22.3 %collective-permute-start = (bf16[1536,256]{1,0:T(8,128)(2,1)S(1)}, bf16[1536,256]{1,0:T(8,128)(2,1)S(1)}, u32[]{:S(2)}, u32[]{:S(2)}) collective-permute-start(bf16[1536,256]{1,0:T(8,128)(2,1)S(1)} %get-tuple-element.21), channel_id=1, source_target_pairs={{0,4},{4,8},{8,12},{12,0},{1,5},{5,9},{9,13},{13,1},{2,6},{6,10},{... | collective-permute-start | bytes 2359304 | tf_op jit(solution)/shard_map/ppermute | solution.py:280
  61.8 23.9 %collective-permute-start.1 = (bf16[1536,256]{1,0:T(8,128)(2,1)S(1)}, bf16[1536,256]{1,0:T(8,128)(2,1)S(1)}, u32[]{:S(2)}, u32[]{:S(2)}) collective-permute-start(bf16[1536,256]{1,0:T(8,128)(2,1)S(1)} %get-tuple-element.22), channel_id=1, source_target_pairs={{0,8},{4,12},{8,0},{12,4},{1,9},{5,13},{9,1},{13,5},{2,10},{6,14},... | collective-permute-start | bytes 2359304 | tf_op jit(solution)/shard_map/ppermute | solution.py:280
  64.7 37.1 %collective-permute-start.2 = (bf16[1536,256]{1,0:T(8,128)(2,1)S(1)}, bf16[1536,256]{1,0:T(8,128)(2,1)S(1)}, u32[]{:S(2)}, u32[]{:S(2)}) collective-permute-start(bf16[1536,256]{1,0:T(8,128)(2,1)S(1)} %get-tuple-element.23), channel_id=1, source_target_pairs={{0,12},{4,0},{8,4},{12,8},{1,13},{5,1},{9,5},{13,9},{2,14},{6,2},{... | collective-permute-start | bytes 2359304 | tf_op jit(solution)/shard_map/ppermute | solution.py:280
  85.7 0.9 copy-start
  101.7 0.9 copy-start.3
  102.7 1.1 copy-start.1
  103.8 1.1 copy-start.4
  130.6 15.4 %copy-start.2 = (bf16[1536,256]{1,0:T(8,128)(2,1)S(1)}, bf16[1536,256]{1,0:T(8,128)(2,1)}, u32[]{:S(2)}) copy-start(bf16[1536,256]{1,0:T(8,128)(2,1)} %copy-done) | copy-start | bytes 2359300
  130.6 15.4 %copy-start.5 = (bf16[1536,256]{1,0:T(8,128)(2,1)S(1)}, bf16[1536,256]{1,0:T(8,128)(2,1)}, u32[]{:S(2)}) copy-start(bf16[1536,256]{1,0:T(8,128)(2,1)} %copy-done.3) | copy-start | bytes 2359300
  148.1 5.1 %copy-start.19 = (bf16[2,256,128]{2,1,0:T(8,128)(2,1)S(1)}, bf16[2,256,128]{2,1,0:T(8,128)(2,1)}, u32[]{:S(2)}) copy-start(bf16[2,256,128]{2,1,0:T(8,128)(2,1)} %copy-done.18) | copy-start | bytes 393220
  148.1 24.7 %all-to-all-start.4 = ((bf16[8,384,256]{2,1,0:T(8,128)(2,1)}), bf16[8,384,256]{2,1,0:T(8,128)(2,1)S(1)}, u32[]{:S(2)}, u32[]{:S(2)}) async-start(bf16[8,384,256]{2,1,0:T(8,128)(2,1)} %bitcast.13), calls=%async_computation.4 | async-start | bytes 3145728 | tf_op jit(solution)/shard_map/all_to_all | solution.py:284
  153.2 1.6 copy-start.17
  166.6 37.0 %copy-start.14 = (s32[256,2]{0,1:T(2,128)S(1)}, s32[256,2]{0,1:T(2,128)}, u32[]{:S(2)}) copy-start(s32[256,2]{0,1:T(2,128)} %param.18) | copy-start | bytes 6148
  166.6 37.0 %copy-start.15 = (f32[256,2]{0,1:T(2,128)S(1)}, f32[256,2]{0,1:T(2,128)}, u32[]{:S(2)}) copy-start(f32[256,2]{0,1:T(2,128)} %param.20) | copy-start | bytes 6148
  166.6 37.0 %copy-start.16 = (f32[256]{0:T(256)S(1)}, f32[256]{0:T(256)}, u32[]{:S(2)}) copy-start(f32[256]{0:T(256)} %param.19) | copy-start | bytes 3076
Sparse Core Ops, SparseCore 0:
  58.2 67.2 all-gather.1
where the time goes:
time: 213 us; the launch traced here: 212 us
  blocking collectives  68.6 us (32%)
  waiting for transfers between devices  59 us (28%)
  starting transfers between devices  35.4 us (17%)
  Pallas kernels  20.5 us (10%)
  between operations  14.3 us (7%)
  local copies, waits for them, and re-layouts  11.8 us (6%)
  other arithmetic  2.21 us (1%)
    all_to_all x3, blocking collectives, exchange(): return lax.all_to_all(a, axes, split_axis=0, concat_axis=0, tiled=True)  68.6 us
    ppermute x3, waiting for transfers between devices, shifted(): lax.ppermute(b, axis, [(i, (i + s) % 4) for i in range(4)])  31.8 us
    all_to_all x3, waiting for transfers between devices, exchange(): return lax.all_to_all(a, axes, split_axis=0, concat_axis=0, tiled=True)  26.5 us
    all_to_all x3, starting transfers between devices, exchange(): return lax.all_to_all(a, axes, split_axis=0, concat_axis=0, tiled=True)  24.7 us
    pallas_call x10, Pallas kernels, call(): pl.pallas_call(kernel, out_shape=outs, in_specs=[spec(a) for a in args],...  20.5 us
    ppermute x3, starting transfers between devices, shifted(): lax.ppermute(b, axis, [(i, (i + s) % 4) for i in range(4)])  10.7 us
    unnamed x40, local copies, waits for them, and re-layouts  10.4 us
  transfers between devices with their start and end apart: 7, of which 5 were waited for; matrix products, arithmetic and copies ran while one was open for 1% of the time, Pallas kernels for 8%

commit v1 on v0

--- a/solution.py
+++ b/solution.py
@@ -85,16 +85,18 @@
     return jnp.concatenate(parts, axis=0)
 
 
-def rope_fn(queries, keys_t, values_t, table):
+def query_fn(queries, table):
     q_t = queries.astype(F32).T
-    q_gain, k_gain = table[64:128], table[128:192]
     heads = []
-    for h in range(4):
-        turned = rotated(q_t[h * HEAD_DIM : (h + 1) * HEAD_DIM], q_gain, table) * 0.125
+    for h in range(2):
+        turned = rotated(q_t[h * HEAD_DIM : (h + 1) * HEAD_DIM], table[64:128], table) * 0.125
         heads.append(jnp.concatenate([turned, jnp.zeros_like(turned)], axis=0).T.astype(BF))
-    k = rotated(keys_t.astype(F32), k_gain, table)
-    kv = jnp.concatenate([k, values_t.astype(F32)], axis=0).T.astype(BF)
-    return heads, kv
+    return heads
+
+
+def key_fn(keys_t, values_t, table):
+    k = rotated(keys_t.astype(F32), table[128:192], table)
+    return jnp.concatenate([k, values_t.astype(F32)], axis=0).T.astype(BF)
 
 
 def gate_up_fn(get_tokens, get_weight, put):
@@ -163,12 +165,13 @@
     out[...] = combine_fn(ids[...], gw[...], ew[...], res[...])
 
 
-def rope_kernel(q, k, v, table, q_first, q_second, kv_out):
-    heads, kv = rope_fn(q[...], k[...], v[...], table[...])
-    for h in range(2):
-        q_first[h] = heads[h]
-        q_second[h] = heads[2 + h]
-    kv_out[...] = kv
+def query_kernel(q, table, out):
+    for h, head in enumerate(query_fn(q[...], table[...])):
+        out[h] = head
+
+
+def key_kernel(k, v, table, out):
+    out[...] = key_fn(k[...], v[...], table[...])
 
 
 def pack_kernel(at, gate, up, down, *outs):
@@ -218,8 +221,8 @@
 KEYS = 1024
 
 
-def attend_kernel(q, kv, out, scores):
-    blocks = [(kv, i) for i in range(kv.shape[0] // KEYS)]
+def attend_kernel(q, own, other, out, scores):
+    blocks = [(ref, i) for ref in (own, other) for i in range(ref.shape[0] // KEYS)]
 
     def lanes(v, op):
         parts = [v[:, 128 * i : 128 * (i + 1)] for i in range(v.shape[1] // 128)]
@@ -295,9 +298,18 @@
     )
 
 
-def attend(q, kv):
-    scratch = [pltpu.VMEM((2, TOK, kv.shape[0]), F32)]
-    return call(attend_kernel, array(TOK, 128), q, kv, flops=2200 << 20, scratch=scratch, vmem=36)
+def attend(q, own, other):
+    scratch = [pltpu.VMEM((2, TOK, 2 * own.shape[0]), F32)]
+    return call(attend_kernel, array(TOK, 128), q, own, other, flops=2200 << 20, scratch=scratch, vmem=36)
+
+
+def spread(kv, shifts):
+    moved = [lax.ppermute(kv, "z", [(i, (i + n) % 16) for i in range(16)]) for n in shifts]
+    return jnp.concatenate([kv, *moved], axis=0)
+
+
+def rotate_queries(q, table):
+    return call(query_kernel, array(2, TOK, 128), q, table, flops=2 << 20)
 
 
 def on_device(
@@ -319,20 +331,13 @@
     routed = call(route_kernel, array(SLOTS, 256), ids, moe_rows, flops=4 << 20)
     arrived = exchange(routed.reshape(16, 2 * CAP, 256), "z")
     table = rope_table(query_gain, key_gain)
-    *q_heads, kv = call(
-        rope_kernel,
-        (array(2, TOK, 128),) * 2 + (array(TOK, 128),),
-        queries,
-        keys.T,
-        values.T,
-        table,
-        flops=4 << 20,
-    )
-    kv = lax.all_gather(kv, EP, axis=0, tiled=True)
+    kv = call(key_kernel, array(TOK, 128), keys.T, values.T, table, flops=2 << 20)
     at = lax.axis_index("y").astype(jnp.int32).reshape(1)
     packed = call(pack_kernel, (array(1536, 256),) * 4, at, expert_gate[0], expert_up[0], expert_down[0])
     weights = shifted(packed, "y")
-    arrived, q_heads = tie((arrived, q_heads))
+    arrived, kv, table = tie((arrived, kv, table))
+    kv = spread(spread(kv, (4, 8, -4)), (1, 2, -1))
+    q_heads = [rotate_queries(queries[:, :128], table), rotate_queries(queries[:, 128:], table)]
     sent = arrived.reshape(16, 2, CAP, 256).transpose(1, 0, 2, 3).reshape(2, 1, HALF, 256)
     tokens = exchange(jnp.broadcast_to(sent, (2, 4, HALF, 256)).reshape(8, HALF, 256), CX)
     partial = call(
@@ -348,7 +353,8 @@
     ).reshape(8, HALF, 256)
     results, q_heads = tie((results, q_heads))
     summands = exchange(results, CY)
-    attended = jnp.concatenate([attend(q, kv) for q in q_heads], axis=1)
+    other = lax.ppermute(kv, "c", [(0, 1), (1, 0)])
+    attended = jnp.concatenate([attend(q, kv, other) for q in q_heads], axis=1)
     summands, attended = tie((summands, attended))
     reduced = call(reduce_kernel, array(16, 2, CAP, 256), summands, flops=4 << 20)
     returned = exchange(reduced.reshape(16, 2 * CAP, 256), "z")

time: 213 us -> 226 us (1.061)
  the two profiles are of different devices: /device:TPU:8 before, /device:TPU:2 now
where the time goes in v1:
time: 226 us; the launch traced here: 225 us
  starting transfers between devices  73.6 us (33%)
  waiting for transfers between devices  67.8 us (30%)
  blocking collectives  33.6 us (15%)
  Pallas kernels  24.2 us (11%)
  local copies, waits for them, and re-layouts  20.2 us (9%)
  other arithmetic  4.89 us (2%)
    all_to_all x5, starting transfers between devices, exchange(): return lax.all_to_all(a, axes, split_axis=0, concat_axis=0, tiled=True)  34.5 us
    all_to_all x1, blocking collectives, exchange(): return lax.all_to_all(a, axes, split_axis=0, concat_axis=0, tiled=True)  33.6 us
    ppermute x3, waiting for transfers between devices, shifted(): lax.ppermute(b, axis, [(i, (i + s) % 4) for i in range(4)])  29.6 us
    all_to_all x5, waiting for transfers between devices, exchange(): return lax.all_to_all(a, axes, split_axis=0, concat_axis=0, tiled=True)  27.8 us
    ppermute x6, starting transfers between devices, spread(): lax.ppermute(kv, 'z', [(i, (i + n) % 16) for i in range(16)])  25.6 us
    pallas_call x12, Pallas kernels, call(): pl.pallas_call(kernel, out_shape=outs, in_specs=[spec(a) for a in args],...  24.2 us
    unnamed x43, local copies, waits for them, and re-layouts  16.5 us
    ppermute x3, starting transfers between devices, shifted(): lax.ppermute(b, axis, [(i, (i + s) % 4) for i in range(4)])  11.6 us
  transfers between devices with their start and end apart: 15, of which 8 were waited for; matrix products, arithmetic and copies ran while one was open for 5% of the time, Pallas kernels for 9%

profile of v1, /device:TPU:2, one launch (start us, length us, event | category | flops | bytes accessed | tf_op | source)
XLA Modules:
  0.0 225.2 jit_solution(11183484232939641851)
XLA Ops:
  3.4 15.2 %all-to-all-start = ((bf16[16,48,256]{2,1,0:T(8,128)(2,1)}), bf16[16,48,256]{2,1,0:T(8,128)(2,1)S(1)}, u32[]{:S(2)}, u32[]{:S(2)}) async-start(bf16[16,48,256]{2,1,0:T(8,128)(2,1)} %bitcast.2), calls=%async_computation | async-start | bytes 786432 | tf_op jit(solution)/shard_map/all_to_all | solution.py:287
  20.0 22.5 %all-to-all-done = bf16[16,48,256]{2,1,0:T(8,128)(2,1)S(1)} async-done(((bf16[16,48,256]{2,1,0:T(8,128)(2,1)}), bf16[16,48,256]{2,1,0:T(8,128)(2,1)S(1)}, u32[]{:S(2)}, u32[]{:S(2)}) %all-to-all-start) | async-done | bytes 393248 | tf_op jit(solution)/shard_map/all_to_all | solution.py:287
  43.7 4.8 %all-to-all-start.1 = ((bf16[8,384,256]{2,1,0:T(8,128)(2,1)}), bf16[8,384,256]{2,1,0:T(8,128)(2,1)S(1)}, u32[]{:S(2)}, u32[]{:S(2)}) async-start(bf16[8,384,256]{2,1,0:T(8,128)(2,1)} %bitcast.9), calls=%async_computation.1 | async-start | bytes 3145728 | tf_op jit(solution)/shard_map/all_to_all | solution.py:287
  52.7 3.5 %collective-permute-start = (bf16[1536,256]{1,0:T(8,128)(2,1)S(1)}, bf16[1536,256]{1,0:T(8,128)(2,1)S(1)}, u32[]{:S(2)}, u32[]{:S(2)}) collective-permute-start(bf16[1536,256]{1,0:T(8,128)(2,1)S(1)} %get-tuple-element.16), channel_id=1, source_target_pairs={{0,4},{4,8},{8,12},{12,0},{1,5},{5,9},{9,13},{13,1},{2,6},{6,10},{... | collective-permute-start | bytes 2359304 | tf_op jit(solution)/shard_map/ppermute | solution.py:283
  56.2 4.8 %collective-permute-start.1 = (bf16[1536,256]{1,0:T(8,128)(2,1)S(1)}, bf16[1536,256]{1,0:T(8,128)(2,1)S(1)}, u32[]{:S(2)}, u32[]{:S(2)}) collective-permute-start(bf16[1536,256]{1,0:T(8,128)(2,1)S(1)} %get-tuple-element.17), channel_id=1, source_target_pairs={{0,8},{4,12},{8,0},{12,4},{1,9},{5,13},{9,1},{13,5},{2,10},{6,14},... | collective-permute-start | bytes 2359304 | tf_op jit(solution)/shard_map/ppermute | solution.py:283
  61.0 3.3 %collective-permute-start.2 = (bf16[1536,256]{1,0:T(8,128)(2,1)S(1)}, bf16[1536,256]{1,0:T(8,128)(2,1)S(1)}, u32[]{:S(2)}, u32[]{:S(2)}) collective-permute-start(bf16[1536,256]{1,0:T(8,128)(2,1)S(1)} %get-tuple-element.18), channel_id=1, source_target_pairs={{0,12},{4,0},{8,4},{12,8},{1,13},{5,1},{9,5},{13,9},{2,14},{6,2},{... | collective-permute-start | bytes 2359304 | tf_op jit(solution)/shard_map/ppermute | solution.py:283
  64.2 11.2 %collective-permute-done.w1 = bf16[1536,256]{1,0:T(8,128)(2,1)S(1)} collective-permute-done((bf16[1536,256]{1,0:T(8,128)(2,1)S(1)}, bf16[1536,256]{1,0:T(8,128)(2,1)S(1)}, u32[]{:S(2)}, u32[]{:S(2)}) %collective-permute-start) | collective-permute-done | bytes 786464 | tf_op jit(solution)/shard_map/ppermute | solution.py:283
  75.4 18.0 %collective-permute-done.1.w2 = bf16[1536,256]{1,0:T(8,128)(2,1)S(1)} collective-permute-done((bf16[1536,256]{1,0:T(8,128)(2,1)S(1)}, bf16[1536,256]{1,0:T(8,128)(2,1)S(1)}, u32[]{:S(2)}, u32[]{:S(2)}) %collective-permute-start.1) | collective-permute-done | bytes 786464 | tf_op jit(solution)/shard_map/ppermute | solution.py:283
  98.0 2.3 %shard_map.134 = f32[4,776,256]{2,1,0:T(8,128)S(1)} custom-call(s32[1]{0:T(128)} %bitcast.at, bf16[8,384,256]{2,1,0:T(8,128)(2,1)S(1)} %all-to-all-done.1.tokens, bf16[1536,256]{1,0:T(8,128)(2,1)S(1)} %get-tuple-element.15.w0, bf16[1536,256]{1,0:T(8,128)(2,1)S(1)} %collective-permute-done.w1, bf16[1536,256]{1,0:T(8,128)(2,1)S(1)} %copy-done.1, ...), custom_call_target="tpu_custom_call" | custom-call | flops 1677721600 | tf_op jit(solution)/shard_map/pallas_call | solution.py:267
  100.2 1.4 convert_element_type.14
  101.7 4.4 %all-to-all-start.2 = ((f16[4,776,256]{2,1,0:T(8,128)(2,1)}), f16[4,776,256]{2,1,0:T(8,128)(2,1)}, u32[]{:S(2)}, u32[]{:S(2)}) async-start(f16[4,776,256]{2,1,0:T(8,128)(2,1)} %convert_element_type.14), calls=%async_computation.2 | async-start | bytes 3178496 | tf_op jit(solution)/shard_map/all_to_all | solution.py:287
  106.1 5.8 %collective-permute-start.3 = (bf16[256,128]{1,0:T(8,128)(2,1)S(1)}, bf16[256,128]{1,0:T(8,128)(2,1)S(1)}, u32[]{:S(2)}, u32[]{:S(2)}) collective-permute-start(bf16[256,128]{1,0:T(8,128)(2,1)S(1)} %shard_map.132), channel_id=1, source_target_pairs={{0,128},{32,160},{64,192},{96,224},{128,256},{160,288},{192,320},{... | collective-permute-start | bytes 196616 | tf_op jit(solution)/shard_map/ppermute | solution.py:307
  111.8 7.2 %collective-permute-start.4 = (bf16[256,128]{1,0:T(8,128)(2,1)S(1)}, bf16[256,128]{1,0:T(8,128)(2,1)S(1)}, u32[]{:S(2)}, u32[]{:S(2)}) collective-permute-start(bf16[256,128]{1,0:T(8,128)(2,1)S(1)} %shard_map.132), channel_id=1, source_target_pairs={{0,256},{32,288},{64,320},{96,352},{128,384},{160,416},{192,448},{... | collective-permute-start | bytes 196616 | tf_op jit(solution)/shard_map/ppermute | solution.py:307
  119.0 3.3 %collective-permute-start.5 = (bf16[256,128]{1,0:T(8,128)(2,1)S(1)}, bf16[256,128]{1,0:T(8,128)(2,1)S(1)}, u32[]{:S(2)}, u32[]{:S(2)}) collective-permute-start(bf16[256,128]{1,0:T(8,128)(2,1)S(1)} %shard_map.132), channel_id=1, source_target_pairs={{0,384},{32,416},{64,448},{96,480},{128,0},{160,32},{192,64},{224,... | collective-permute-start | bytes 196616 | tf_op jit(solution)/shard_map/ppermute | solution.py:307
  123.7 4.7 %collective-permute-done.4 = bf16[256,128]{1,0:T(8,128)(2,1)S(1)} collective-permute-done((bf16[256,128]{1,0:T(8,128)(2,1)S(1)}, bf16[256,128]{1,0:T(8,128)(2,1)S(1)}, u32[]{:S(2)}, u32[]{:S(2)}) %collective-permute-start.4) | collective-permute-done | bytes 65568 | tf_op jit(solution)/shard_map/ppermute | solution.py:307
  129.1 4.7 %collective-permute-done.5 = bf16[256,128]{1,0:T(8,128)(2,1)S(1)} collective-permute-done((bf16[256,128]{1,0:T(8,128)(2,1)S(1)}, bf16[256,128]{1,0:T(8,128)(2,1)S(1)}, u32[]{:S(2)}, u32[]{:S(2)}) %collective-permute-start.5) | collective-permute-done | bytes 65568 | tf_op jit(solution)/shard_map/ppermute | solution.py:307
  134.4 1.9 collective-permute-start.6
  136.3 2.7 %collective-permute-start.7 = (bf16[1024,128]{1,0:T(8,128)(2,1)}, bf16[1024,128]{1,0:T(8,128)(2,1)}, u32[]{:S(2)}, u32[]{:S(2)}) collective-permute-start(bf16[1024,128]{1,0:T(8,128)(2,1)} %get-tuple-element.28), channel_id=1, source_target_pairs={{0,64},{32,96},{64,128},{96,160},{128,192},{160,224},{192,256},{22... | collective-permute-start | bytes 786440 | tf_op jit(solution)/shard_map/ppermute | solution.py:307
  139.1 4.7 %collective-permute-start.8 = (bf16[1024,128]{1,0:T(8,128)(2,1)}, bf16[1024,128]{1,0:T(8,128)(2,1)}, u32[]{:S(2)}, u32[]{:S(2)}) collective-permute-start(bf16[1024,128]{1,0:T(8,128)(2,1)} %get-tuple-element.28), channel_id=1, source_target_pairs={{0,480},{32,0},{64,32},{96,64},{128,96},{160,128},{192,160},{224,1... | collective-permute-start | bytes 786440 | tf_op jit(solution)/shard_map/ppermute | solution.py:307
  143.8 1.7 convert_reduce_fusion.parts
  146.8 4.9 %all-to-all-start.3 = ((bf16[4,768,128]{2,1,0:T(8,128)(2,1)}), bf16[4,768,128]{2,1,0:T(8,128)(2,1)S(1)}, u32[]{:S(2)}, u32[]{:S(2)}) async-start(bf16[4,768,128]{2,1,0:T(8,128)(2,1)} %shard_map.135), calls=%async_computation.3 | async-start | bytes 1572864 | tf_op jit(solution)/shard_map/all_to_all | solution.py:287
  152.6 1.7 constant_dynamic-update-slice_fusion.6
  154.3 1.7 constant_dynamic-update-slice_fusion.5
  156.0 1.7 constant_dynamic-update-slice_fusion.4.own
  157.7 1.9 collective-permute-start.9
  161.9 2.2 shard_map.136
  164.1 5.1 %all-to-all-start.4 = ((bf16[8,384,256]{2,1,0:T(8,128)(2,1)}), bf16[8,384,256]{2,1,0:T(8,128)(2,1)S(1)}, u32[]{:S(2)}, u32[]{:S(2)}) async-start(bf16[8,384,256]{2,1,0:T(8,128)(2,1)} %bitcast.13), calls=%async_computation.4 | async-start | bytes 3145728 | tf_op jit(solution)/shard_map/all_to_all | solution.py:287
  169.2 7.4 %shard_map.140 = bf16[256,128]{1,0:T(8,128)(2,1)S(1)} custom-call(bf16[2,256,128]{2,1,0:T(8,128)(2,1)S(1)} %copy-done.10, bf16[4096,128]{1,0:T(8,128)(2,1)} %constant_dynamic-update-slice_fusion.4.own, bf16[4096,128]{1,0:T(8,128)(2,1)} %collective-permute-done.9.other), custom_call_target="tpu_custom_call" | custom-call | flops 2306867200 | tf_op jit(solution)/shard_map/pallas_call | solution.py:267
  176.6 7.4 %shard_map.139 = bf16[256,128]{1,0:T(8,128)(2,1)S(1)} custom-call(bf16[2,256,128]{2,1,0:T(8,128)(2,1)S(1)} %shard_map.137.q, bf16[4096,128]{1,0:T(8,128)(2,1)} %constant_dynamic-update-slice_fusion.4.own, bf16[4096,128]{1,0:T(8,128)(2,1)} %collective-permute-done.9.other), custom_call_target="tpu_custom_call" | custom-call | flops 2306867200 | tf_op jit(solution)/shard_map/pallas_call | solution.py:267
  184.8 5.3 %all-to-all-done.4.parts = bf16[8,384,256]{2,1,0:T(8,128)(2,1)S(1)} async-done(((bf16[8,384,256]{2,1,0:T(8,128)(2,1)}), bf16[8,384,256]{2,1,0:T(8,128)(2,1)S(1)}, u32[]{:S(2)}, u32[]{:S(2)}) %all-to-all-start.4) | async-done | bytes 1572896 | tf_op jit(solution)/shard_map/all_to_all | solution.py:287
  190.3 33.6 %all_to_all.30 = bf16[16,48,256]{2,1,0:T(8,128)(2,1)S(1)} all-to-all(bf16[16,48,256]{2,1,0:T(8,128)(2,1)S(1)} %bitcast.25), channel_id=1, replica_groups=mesh['z'=16,'c'=2,'y'=4,'x'=4] {'z'}, dimensions={0} | all-to-all | bytes 786432 | tf_op jit(solution)/shard_map/all_to_all | solution.py:287
  223.9 1.3 shard_map.142
  (70 shorter events, 22.0 us)
Async XLA Ops:
  0.6 0.9 copy-start.11
  2.2 17.6 %copy-start.12 = (bf16[256,64]{0,1:T(8,128)(2,1)S(1)}, bf16[256,64]{0,1:T(8,128)(2,1)}, u32[]{:S(2)}) copy-start(bf16[256,64]{0,1:T(8,128)(2,1)} %param.13) | copy-start | bytes 98308
  2.2 17.6 %copy-start.13 = (bf16[256,64]{0,1:T(8,128)(2,1)S(1)}, bf16[256,64]{0,1:T(8,128)(2,1)}, u32[]{:S(2)}) copy-start(bf16[256,64]{0,1:T(8,128)(2,1)} %param.14) | copy-start | bytes 98308
  3.4 39.0 %all-to-all-start = ((bf16[16,48,256]{2,1,0:T(8,128)(2,1)}), bf16[16,48,256]{2,1,0:T(8,128)(2,1)S(1)}, u32[]{:S(2)}, u32[]{:S(2)}) async-start(bf16[16,48,256]{2,1,0:T(8,128)(2,1)} %bitcast.2), calls=%async_computation | async-start | bytes 786432 | tf_op jit(solution)/shard_map/all_to_all | solution.py:287
  43.7 52.0 %all-to-all-start.1 = ((bf16[8,384,256]{2,1,0:T(8,128)(2,1)}), bf16[8,384,256]{2,1,0:T(8,128)(2,1)S(1)}, u32[]{:S(2)}, u32[]{:S(2)}) async-start(bf16[8,384,256]{2,1,0:T(8,128)(2,1)} %bitcast.9), calls=%async_computation.1 | async-start | bytes 3145728 | tf_op jit(solution)/shard_map/all_to_all | solution.py:287
  48.6 1.2 copy-start.6
  49.8 1.2 copy-start.7
  51.0 1.2 copy-start.8
  52.7 22.7 %collective-permute-start = (bf16[1536,256]{1,0:T(8,128)(2,1)S(1)}, bf16[1536,256]{1,0:T(8,128)(2,1)S(1)}, u32[]{:S(2)}, u32[]{:S(2)}) collective-permute-start(bf16[1536,256]{1,0:T(8,128)(2,1)S(1)} %get-tuple-element.16), channel_id=1, source_target_pairs={{0,4},{4,8},{8,12},{12,0},{1,5},{5,9},{9,13},{13,1},{2,6},{6,10},{... | collective-permute-start | bytes 2359304 | tf_op jit(solution)/shard_map/ppermute | solution.py:283
  56.2 37.3 %collective-permute-start.1 = (bf16[1536,256]{1,0:T(8,128)(2,1)S(1)}, bf16[1536,256]{1,0:T(8,128)(2,1)S(1)}, u32[]{:S(2)}, u32[]{:S(2)}) collective-permute-start(bf16[1536,256]{1,0:T(8,128)(2,1)S(1)} %get-tuple-element.17), channel_id=1, source_target_pairs={{0,8},{4,12},{8,0},{12,4},{1,9},{5,13},{9,1},{13,5},{2,10},{6,14},... | collective-permute-start | bytes 2359304 | tf_op jit(solution)/shard_map/ppermute | solution.py:283
  61.0 33.8 %collective-permute-start.2 = (bf16[1536,256]{1,0:T(8,128)(2,1)S(1)}, bf16[1536,256]{1,0:T(8,128)(2,1)S(1)}, u32[]{:S(2)}, u32[]{:S(2)}) collective-permute-start(bf16[1536,256]{1,0:T(8,128)(2,1)S(1)} %get-tuple-element.18), channel_id=1, source_target_pairs={{0,12},{4,0},{8,4},{12,8},{1,13},{5,1},{9,5},{13,9},{2,14},{6,2},{... | collective-permute-start | bytes 2359304 | tf_op jit(solution)/shard_map/ppermute | solution.py:283
  93.4 0.9 copy-start
  94.8 0.9 copy-start.3
  95.7 1.1 copy-start.1
  96.8 1.1 copy-start.4
  101.7 42.2 %all-to-all-start.2 = ((f16[4,776,256]{2,1,0:T(8,128)(2,1)}), f16[4,776,256]{2,1,0:T(8,128)(2,1)}, u32[]{:S(2)}, u32[]{:S(2)}) async-start(f16[4,776,256]{2,1,0:T(8,128)(2,1)} %convert_element_type.14), calls=%async_computation.2 | async-start | bytes 3178496 | tf_op jit(solution)/shard_map/all_to_all | solution.py:287
  106.1 16.9 %collective-permute-start.3 = (bf16[256,128]{1,0:T(8,128)(2,1)S(1)}, bf16[256,128]{1,0:T(8,128)(2,1)S(1)}, u32[]{:S(2)}, u32[]{:S(2)}) collective-permute-start(bf16[256,128]{1,0:T(8,128)(2,1)S(1)} %shard_map.132), channel_id=1, source_target_pairs={{0,128},{32,160},{64,192},{96,224},{128,256},{160,288},{192,320},{... | collective-permute-start | bytes 196616 | tf_op jit(solution)/shard_map/ppermute | solution.py:307
  111.8 16.6 %collective-permute-start.4 = (bf16[256,128]{1,0:T(8,128)(2,1)S(1)}, bf16[256,128]{1,0:T(8,128)(2,1)S(1)}, u32[]{:S(2)}, u32[]{:S(2)}) collective-permute-start(bf16[256,128]{1,0:T(8,128)(2,1)S(1)} %shard_map.132), channel_id=1, source_target_pairs={{0,256},{32,288},{64,320},{96,352},{128,384},{160,416},{192,448},{... | collective-permute-start | bytes 196616 | tf_op jit(solution)/shard_map/ppermute | solution.py:307
  119.0 14.7 %collective-permute-start.5 = (bf16[256,128]{1,0:T(8,128)(2,1)S(1)}, bf16[256,128]{1,0:T(8,128)(2,1)S(1)}, u32[]{:S(2)}, u32[]{:S(2)}) collective-permute-start(bf16[256,128]{1,0:T(8,128)(2,1)S(1)} %shard_map.132), channel_id=1, source_target_pairs={{0,384},{32,416},{64,448},{96,480},{128,0},{160,32},{192,64},{224,... | collective-permute-start | bytes 196616 | tf_op jit(solution)/shard_map/ppermute | solution.py:307
  134.4 18.2 %collective-permute-start.6 = (bf16[1024,128]{1,0:T(8,128)(2,1)}, bf16[1024,128]{1,0:T(8,128)(2,1)}, u32[]{:S(2)}, u32[]{:S(2)}) collective-permute-start(bf16[1024,128]{1,0:T(8,128)(2,1)} %get-tuple-element.28), channel_id=1, source_target_pairs={{0,32},{32,64},{64,96},{96,128},{128,160},{160,192},{192,224},{224... | collective-permute-start | bytes 786440 | tf_op jit(solution)/shard_map/ppermute | solution.py:307
  136.3 17.9 %collective-permute-start.7 = (bf16[1024,128]{1,0:T(8,128)(2,1)}, bf16[1024,128]{1,0:T(8,128)(2,1)}, u32[]{:S(2)}, u32[]{:S(2)}) collective-permute-start(bf16[1024,128]{1,0:T(8,128)(2,1)} %get-tuple-element.28), channel_id=1, source_target_pairs={{0,64},{32,96},{64,128},{96,160},{128,192},{160,224},{192,256},{22... | collective-permute-start | bytes 786440 | tf_op jit(solution)/shard_map/ppermute | solution.py:307
  139.1 16.9 %collective-permute-start.8 = (bf16[1024,128]{1,0:T(8,128)(2,1)}, bf16[1024,128]{1,0:T(8,128)(2,1)}, u32[]{:S(2)}, u32[]{:S(2)}) collective-permute-start(bf16[1024,128]{1,0:T(8,128)(2,1)} %get-tuple-element.28), channel_id=1, source_target_pairs={{0,480},{32,0},{64,32},{96,64},{128,96},{160,128},{192,160},{224,1... | collective-permute-start | bytes 786440 | tf_op jit(solution)/shard_map/ppermute | solution.py:307
  146.8 12.8 %copy-start.18 = (bf16[256,256]{1,0:T(8,128)(2,1)S(1)}, bf16[256,256]{1,0:T(8,128)(2,1)}, u32[]{:S(2)}) copy-start(bf16[256,256]{1,0:T(8,128)(2,1)} %param.12) | copy-start | bytes 393220
  146.8 14.0 %all-to-all-start.3 = ((bf16[4,768,128]{2,1,0:T(8,128)(2,1)}), bf16[4,768,128]{2,1,0:T(8,128)(2,1)S(1)}, u32[]{:S(2)}, u32[]{:S(2)}) async-start(bf16[4,768,128]{2,1,0:T(8,128)(2,1)} %shard_map.135), calls=%async_computation.3 | async-start | bytes 1572864 | tf_op jit(solution)/shard_map/all_to_all | solution.py:287
  151.7 9.1 %copy-start.2 = (bf16[1536,256]{1,0:T(8,128)(2,1)S(1)}, bf16[1536,256]{1,0:T(8,128)(2,1)}, u32[]{:S(2)}) copy-start(bf16[1536,256]{1,0:T(8,128)(2,1)} %copy-done) | copy-start | bytes 2359300
  157.7 11.5 %collective-permute-start.9 = (bf16[4096,128]{1,0:T(8,128)(2,1)}, bf16[4096,128]{1,0:T(8,128)(2,1)}, u32[]{:S(2)}, u32[]{:S(2)}) collective-permute-start(bf16[4096,128]{1,0:T(8,128)(2,1)} %constant_dynamic-update-slice_fusion.4.own), channel_id=1, source_target_pairs={{0,16},{16,0},{1,17},{17,1},{2,18},{18,2},{3,19},{19,3},{4,20},{20... | collective-permute-start | bytes 3145736 | tf_op jit(solution)/shard_map/ppermute | solution.py:356
  160.8 1.1 copy-start.5
  164.0 5.2 %copy-start.10 = (bf16[2,256,128]{2,1,0:T(8,128)(2,1)S(1)}, bf16[2,256,128]{2,1,0:T(8,128)(2,1)}, u32[]{:S(2)}) copy-start(bf16[2,256,128]{2,1,0:T(8,128)(2,1)} %copy-done.9) | copy-start | bytes 393220
  164.1 26.0 %all-to-all-start.4 = ((bf16[8,384,256]{2,1,0:T(8,128)(2,1)}), bf16[8,384,256]{2,1,0:T(8,128)(2,1)S(1)}, u32[]{:S(2)}, u32[]{:S(2)}) async-start(bf16[8,384,256]{2,1,0:T(8,128)(2,1)} %bitcast.13), calls=%async_computation.4 | async-start | bytes 3145728 | tf_op jit(solution)/shard_map/all_to_all | solution.py:287
  184.0 39.8 %copy-start.15 = (s32[256,2]{0,1:T(2,128)S(1)}, s32[256,2]{0,1:T(2,128)}, u32[]{:S(2)}) copy-start(s32[256,2]{0,1:T(2,128)} %param.18) | copy-start | bytes 6148
  184.1 39.8 %copy-start.16 = (f32[256,2]{0,1:T(2,128)S(1)}, f32[256,2]{0,1:T(2,128)}, u32[]{:S(2)}) copy-start(f32[256,2]{0,1:T(2,128)} %param.20) | copy-start | bytes 6148
  184.1 39.8 %copy-start.17 = (f32[256]{0:T(256)S(1)}, f32[256]{0:T(256)}, u32[]{:S(2)}) copy-start(f32[256]{0:T(256)} %param.19) | copy-start | bytes 3076
  (2 other events, 1.3 us)

commit v2 on v0

--- a/solution.py
+++ b/solution.py
@@ -20,8 +20,16 @@
 EXTRA = 8
 EP = ("z", "c")
 TP = ("y", "x")
-CX = ("c", "x")
-CY = ("c", "y")
+ACROSS = ("c", "y", "x")
+
+
+def member(c, r, g):
+    y, x = (r, g) if c == 0 else (g, r)
+    return c * 16 + y * 4 + x
+
+
+GATHER = [[member(c, r, g) for g in range(4)] for c in range(2) for r in range(4)]
+REDUCE = [[member(c, r, g) for r in range(4)] for c in range(2) for g in range(4)]
 BF = jnp.bfloat16
 F32 = jnp.float32
 
@@ -149,10 +157,7 @@
 
 
 def reduce_fn(get):
-    return [
-        sum(get(4 * c + y).astype(F32) for y in range(4)).astype(BF).reshape(16, CAP, 256)
-        for c in range(2)
-    ]
+    return sum(get(r).astype(F32) for r in range(4)).astype(BF)
 
 
 def route_kernel(ids, rows, out):
@@ -173,11 +178,14 @@
 
 def pack_kernel(at, gate, up, down, *outs):
     for s in range(4):
-        y = lax.rem(at[0] + s, 4)
-        rows = pl.ds(pl.multiple_of(y * 1024, 1024), 1024)
-        outs[s][0:1024, 0:128] = gate[rows, :]
-        outs[s][0:1024, 128:256] = up[rows, :]
-        outs[s][1024:1536, :] = down[pl.ds(pl.multiple_of(y * 512, 512), 512), :]
+        r = lax.rem(at[0] + s, 4)
+        for j in range(4):
+            part = r * at[1] + j * at[2]
+            rows = pl.ds(pl.multiple_of(part * 256, 256), 256)
+            outs[s][256 * j : 256 * (j + 1), 0:128] = gate[rows, :]
+            outs[s][256 * j : 256 * (j + 1), 128:256] = up[rows, :]
+            rows = pl.ds(pl.multiple_of(part * 128, 128), 128)
+            outs[s][1024 + 128 * j : 1024 + 128 * (j + 1), :] = down[rows, :]
 
 
 def gate_up_kernel(at, tokens, w0, w1, w2, w3, out):
@@ -186,7 +194,7 @@
     def put(s, row, value):
         out[lax.rem(at[0] + 4 - s, 4), row : row + value.shape[0], :] = value
 
-    gate_up_fn(lambda i: tokens[i], lambda s: weights[s][0:1024, :], put)
+    gate_up_fn(lambda i: tokens[i % 4, i // 4 * HALF : (i // 4 + 1) * HALF, :], lambda s: weights[s][0:1024, :], put)
 
 
 def hidden_kernel(parts, out):
@@ -201,7 +209,7 @@
     weights = (w0, w1, w2, w3)
 
     def put(c, s, value):
-        out[c, lax.rem(at[0] + 4 - s, 4)] = value
+        out[lax.rem(at[0] + 4 - s, 4), c * HALF : (c + 1) * HALF, :] = value
 
     down_fn(
         lambda x, c: hidden[x, c * HALF : (c + 1) * HALF, :],
@@ -211,8 +219,8 @@
 
 
 def reduce_kernel(parts, out):
-    for c, value in enumerate(reduce_fn(lambda i: parts[i])):
-        out[:, c] = value
+    for c in range(2):
+        out[c] = reduce_fn(lambda r: parts[r, c * HALF : (c + 1) * HALF, :])
 
 
 KEYS = 1024
@@ -259,7 +267,7 @@
 
 def call(kernel, outs, *args, flops=0, scratch=(), vmem=20, space=pltpu.VMEM):
     def spec(a):
-        return pl.BlockSpec(memory_space=pltpu.SMEM if a.dtype == jnp.int32 and a.size == 1 else space)
+        return pl.BlockSpec(memory_space=pltpu.SMEM if a.dtype == jnp.int32 and a.size == 3 else space)
 
     return pl.pallas_call(
         kernel,
@@ -276,12 +284,16 @@
     return jax.ShapeDtypeStruct(shape, dtype)
 
 
-def shifted(blocks, axis):
-    return [b if s == 0 else lax.ppermute(b, axis, [(i, (i + s) % 4) for i in range(4)]) for s, b in enumerate(blocks)]
-
-
-def exchange(a, axes):
-    return lax.all_to_all(a, axes, split_axis=0, concat_axis=0, tiled=True)
+def shifted(blocks):
+    out = [blocks[0]]
+    for s in range(1, 4):
+        pairs = [(group[r], group[(r + s) % 4]) for group in REDUCE for r in range(4)]
+        out.append(lax.ppermute(blocks[s], ACROSS, pairs))
+    return out
+
+
+def exchange(a, axes, groups=None):
+    return lax.all_to_all(a, axes, split_axis=0, concat_axis=0, axis_index_groups=groups, tiled=True)
 
 
 def rope_table(query_gain, key_gain):
@@ -329,29 +341,32 @@
         flops=4 << 20,
     )
     kv = lax.all_gather(kv, EP, axis=0, tiled=True)
-    at = lax.axis_index("y").astype(jnp.int32).reshape(1)
+    flip = lax.axis_index("c")
+    y, x = lax.axis_index("y"), lax.axis_index("x")
+    at = jnp.stack([y + flip * (x - y), 4 - 3 * flip, 1 + 3 * flip]).astype(jnp.int32)
     packed = call(pack_kernel, (array(1536, 256),) * 4, at, expert_gate[0], expert_up[0], expert_down[0])
-    weights = shifted(packed, "y")
+    weights = shifted(packed)
     arrived, q_heads = tie((arrived, q_heads))
-    sent = arrived.reshape(16, 2, CAP, 256).transpose(1, 0, 2, 3).reshape(2, 1, HALF, 256)
-    tokens = exchange(jnp.broadcast_to(sent, (2, 4, HALF, 256)).reshape(8, HALF, 256), CX)
+    rows = arrived.reshape(16, 2, CAP, 256).transpose(1, 0, 2, 3).reshape(2, HALF, 256)
+    rows = exchange(rows, "c").reshape(1, SLOTS, 256)
+    tokens = exchange(jnp.broadcast_to(rows, (4, SLOTS, 256)), ACROSS, GATHER)
     partial = call(
         gate_up_kernel, array(4, SLOTS + EXTRA, 256, dtype=F32), at, tokens, *weights, flops=1600 << 20
     ).astype(jnp.float16)
-    products = exchange(partial, "y")
+    products = exchange(partial, ACROSS, REDUCE)
     hidden = call(
         hidden_kernel, array(4, SLOTS, 128), jnp.sum(products.astype(F32), axis=0), flops=8 << 20
     )
-    hidden = exchange(hidden, "x")
-    results = call(
-        down_kernel, array(2, 4, HALF, 256), at, hidden, *weights, flops=800 << 20
-    ).reshape(8, HALF, 256)
-    results, q_heads = tie((results, q_heads))
-    summands = exchange(results, CY)
+    hidden = exchange(hidden, ACROSS, GATHER)
+    results = call(down_kernel, array(4, SLOTS, 256), at, hidden, *weights, flops=800 << 20)
+    summands = exchange(results, ACROSS, REDUCE)
+    reduced = call(reduce_kernel, array(2, HALF, 256), summands, flops=4 << 20)
+    reduced = exchange(reduced, "c")
+    reduced = reduced.reshape(2, 16, CAP, 256).transpose(1, 0, 2, 3).reshape(16, 2 * CAP, 256)
+    reduced, q_heads = tie((reduced, q_heads))
+    returned = exchange(reduced, "z")
     attended = jnp.concatenate([attend(q, kv) for q in q_heads], axis=1)
-    summands, attended = tie((summands, attended))
-    reduced = call(reduce_kernel, array(16, 2, CAP, 256), summands, flops=4 << 20)
-    returned = exchange(reduced.reshape(16, 2 * CAP, 256), "z")
+    returned, attended = tie((returned, attended))
     moe_out = call(
         combine_kernel,
         array(TOK, 256),

time: 213 us -> 202 us (0.948)
  the two profiles are of different devices: /device:TPU:8 before, /device:TPU:1 now
where the time goes in v2:
time: 202 us; the launch traced here: 201 us
  waiting for transfers between devices  62.2 us (31%)
  blocking collectives  44.8 us (22%)
  starting transfers between devices  40.9 us (20%)
  Pallas kernels  21 us (10%)
  between operations  14.3 us (7%)
  local copies, waits for them, and re-layouts  12.6 us (6%)
  other arithmetic  4.97 us (2%)
    all_to_all x4, blocking collectives, exchange(): lax.all_to_all(a, axes, split_axis=0, concat_axis=0, axis_index_groups=gr...  44.8 us
    all_to_all x4, starting transfers between devices, exchange(): lax.all_to_all(a, axes, split_axis=0, concat_axis=0, axis_index_groups=gr...  30.3 us
    all_to_all x4, waiting for transfers between devices, exchange(): lax.all_to_all(a, axes, split_axis=0, concat_axis=0, axis_index_groups=gr...  27.6 us
    pallas_call x10, Pallas kernels, call(): pl.pallas_call(kernel, out_shape=outs, in_specs=[spec(a) for a in args],...  21 us
    all_gather x1, waiting for transfers between devices, on_device(): kv = lax.all_gather(kv, EP, axis=0, tiled=True)  17.7 us
    ppermute x3, waiting for transfers between devices, shifted(): out.append(lax.ppermute(blocks[s], ACROSS, pairs))  16.3 us
    ppermute x3, starting transfers between devices, shifted(): out.append(lax.ppermute(blocks[s], ACROSS, pairs))  10.5 us
    unnamed x40, local copies, waits for them, and re-layouts  10.4 us
  transfers between devices with their start and end apart: 8, of which 5 were waited for; matrix products, arithmetic and copies ran while one was open for 2% of the time, Pallas kernels for 8%

profile of v2, /device:TPU:1, one launch (start us, length us, event | category | flops | bytes accessed | tf_op | source)
XLA Modules:
  0.0 200.7 jit_solution(14299589004756379973)
XLA Ops:
  7.2 0.9 copy-done.10
  8.8 1.2 shard_map.131
  10.0 15.7 %all-to-all-start = ((bf16[16,48,256]{2,1,0:T(8,128)(2,1)}), bf16[16,48,256]{2,1,0:T(8,128)(2,1)S(1)}, u32[]{:S(2)}, u32[]{:S(2)}) async-start(bf16[16,48,256]{2,1,0:T(8,128)(2,1)} %bitcast.4), calls=%async_computation | async-start | bytes 786432 | tf_op jit(solution)/shard_map/all_to_all | solution.py:296
  28.6 15.3 %all-to-all-done = bf16[16,48,256]{2,1,0:T(8,128)(2,1)S(1)} async-done(((bf16[16,48,256]{2,1,0:T(8,128)(2,1)}), bf16[16,48,256]{2,1,0:T(8,128)(2,1)S(1)}, u32[]{:S(2)}, u32[]{:S(2)}) %all-to-all-start) | async-done | bytes 393248 | tf_op jit(solution)/shard_map/all_to_all | solution.py:296
  43.9 10.3 %all_to_all.40 = bf16[2,384,256]{2,1,0:T(8,128)(2,1)S(1)} all-to-all(bf16[2,384,256]{2,1,0:T(8,128)(2,1)S(1)} %bitcast.39), channel_id=1, replica_groups=mesh['z'=16,'c'=2,'y'=4,'x'=4] {'c'}, dimensions={0} | all-to-all | bytes 786432 | tf_op jit(solution)/shard_map/all_to_all | solution.py:296
  54.2 1.3 broadcast_in_dim.8
  55.5 4.3 %all-to-all-start.2 = ((bf16[4,768,256]{2,1,0:T(8,128)(2,1)}), bf16[4,768,256]{2,1,0:T(8,128)(2,1)S(1)}, u32[]{:S(2)}, u32[]{:S(2)}) async-start(bf16[4,768,256]{2,1,0:T(8,128)(2,1)} %broadcast_in_dim.8), calls=%async_computation.2 | async-start | bytes 3145728 | tf_op jit(solution)/shard_map/all_to_all | solution.py:296
  59.9 1.2 copy-done.7
  61.1 1.2 copy-done.8
  62.3 1.0 shard_map.133
  63.3 3.1 %collective-permute-start = (bf16[1536,256]{1,0:T(8,128)(2,1)S(1)}, bf16[1536,256]{1,0:T(8,128)(2,1)S(1)}, u32[]{:S(2)}, u32[]{:S(2)}) collective-permute-start(bf16[1536,256]{1,0:T(8,128)(2,1)S(1)} %get-tuple-element.21), channel_id=1, source_target_pairs={{0,4},{4,8},{8,12},{12,0},{1,5},{5,9},{9,13},{13,1},{2,6},{6,10},{... | collective-permute-start | bytes 2359304 | tf_op jit(solution)/shard_map/ppermute | solution.py:291
  66.4 4.4 %collective-permute-start.1 = (bf16[1536,256]{1,0:T(8,128)(2,1)S(1)}, bf16[1536,256]{1,0:T(8,128)(2,1)S(1)}, u32[]{:S(2)}, u32[]{:S(2)}) collective-permute-start(bf16[1536,256]{1,0:T(8,128)(2,1)S(1)} %get-tuple-element.22), channel_id=1, source_target_pairs={{0,8},{4,12},{8,0},{12,4},{1,9},{5,13},{9,1},{13,5},{2,10},{6,14},... | collective-permute-start | bytes 2359304 | tf_op jit(solution)/shard_map/ppermute | solution.py:291
  70.8 3.1 %collective-permute-start.2 = (bf16[1536,256]{1,0:T(8,128)(2,1)S(1)}, bf16[1536,256]{1,0:T(8,128)(2,1)S(1)}, u32[]{:S(2)}, u32[]{:S(2)}) collective-permute-start(bf16[1536,256]{1,0:T(8,128)(2,1)S(1)} %get-tuple-element.23), channel_id=1, source_target_pairs={{0,12},{4,0},{8,4},{12,8},{1,13},{5,1},{9,5},{13,9},{2,14},{6,2},{... | collective-permute-start | bytes 2359304 | tf_op jit(solution)/shard_map/ppermute | solution.py:291
  73.9 7.9 %collective-permute-done.w1 = bf16[1536,256]{1,0:T(8,128)(2,1)S(1)} collective-permute-done((bf16[1536,256]{1,0:T(8,128)(2,1)S(1)}, bf16[1536,256]{1,0:T(8,128)(2,1)S(1)}, u32[]{:S(2)}, u32[]{:S(2)}) %collective-permute-start) | collective-permute-done | bytes 786464 | tf_op jit(solution)/shard_map/ppermute | solution.py:291
  81.8 8.4 %collective-permute-done.1.w2 = bf16[1536,256]{1,0:T(8,128)(2,1)S(1)} collective-permute-done((bf16[1536,256]{1,0:T(8,128)(2,1)S(1)}, bf16[1536,256]{1,0:T(8,128)(2,1)S(1)}, u32[]{:S(2)}, u32[]{:S(2)}) %collective-permute-start.1) | collective-permute-done | bytes 786464 | tf_op jit(solution)/shard_map/ppermute | solution.py:291
  92.0 1.1 copy-done.1
  93.1 1.1 copy-done.4
  94.2 2.8 %shard_map.134 = f32[4,776,256]{2,1,0:T(8,128)S(1)} custom-call(s32[3]{0:T(128)S(1)} %pad_add_fusion.at, bf16[4,768,256]{2,1,0:T(8,128)(2,1)S(1)} %all-to-all-done.2.tokens, bf16[1536,256]{1,0:T(8,128)(2,1)S(1)} %get-tuple-element.20.w0, bf16[1536,256]{1,0:T(8,128)(2,1)S(1)} %collective-permute-done.w1, bf16[1536,256]{1,0:T(8,128)(2,1)S(1)} %copy-done.1, ...), custom_call_target="tpu_custom_call" | custom-call | flops 1677721600 | tf_op jit(solution)/shard_map/pallas_call | solution.py:272
  97.1 1.4 convert_element_type.14
  98.5 4.4 %all-to-all-start.3 = ((f16[4,776,256]{2,1,0:T(8,128)(2,1)}), f16[4,776,256]{2,1,0:T(8,128)(2,1)}, u32[]{:S(2)}, u32[]{:S(2)}) async-start(f16[4,776,256]{2,1,0:T(8,128)(2,1)} %convert_element_type.14), calls=%async_computation.3 | async-start | bytes 3178496 | tf_op jit(solution)/shard_map/all_to_all | solution.py:296
  103.6 12.3 %all-to-all-done.3 = f16[4,776,256]{2,1,0:T(8,128)(2,1)} async-done(((f16[4,776,256]{2,1,0:T(8,128)(2,1)}), f16[4,776,256]{2,1,0:T(8,128)(2,1)}, u32[]{:S(2)}, u32[]{:S(2)}) %all-to-all-start.3) | async-done | bytes 1589280 | tf_op jit(solution)/shard_map/all_to_all | solution.py:296
  115.9 1.7 convert_reduce_fusion.parts
  117.9 12.5 %all_to_all.41.hidden = bf16[4,768,128]{2,1,0:T(8,128)(2,1)S(1)} all-to-all(bf16[4,768,128]{2,1,0:T(8,128)(2,1)S(1)} %shard_map.135), channel_id=1, replica_groups={{0,1,2,3},{4,5,6,7},{8,9,10,11},{12,13,14,15},{16,20,24,28},{17,21,25,2..., dimensions={0} | all-to-all | bytes 1572864 | tf_op jit(solution)/shard_map/all_to_all | solution.py:296
  130.3 1.5 shard_map.136
  131.9 15.0 %all_to_all.42.parts = bf16[4,768,256]{2,1,0:T(8,128)(2,1)S(1)} all-to-all(bf16[4,768,256]{2,1,0:T(8,128)(2,1)S(1)} %shard_map.136), channel_id=1, replica_groups={{0,4,8,12},{1,5,9,13},{2,6,10,14},{3,7,11,15},{16,17,18,19},{20,21,22,2..., dimensions={0} | all-to-all | bytes 3145728 | tf_op jit(solution)/shard_map/all_to_all | solution.py:296
  147.1 7.0 %all_to_all.43 = bf16[2,384,256]{2,1,0:T(8,128)(2,1)S(1)} all-to-all(bf16[2,384,256]{2,1,0:T(8,128)(2,1)S(1)} %shard_map.137), channel_id=1, replica_groups=mesh['z'=16,'c'=2,'y'=4,'x'=4] {'c'}, dimensions={0} | all-to-all | bytes 786432 | tf_op jit(solution)/shard_map/all_to_all | solution.py:296
  154.9 5.9 %all-to-all-start.7 = ((bf16[16,48,256]{2,1,0:T(8,128)(2,1)}), bf16[16,48,256]{2,1,0:T(8,128)(2,1)S(1)}, u32[]{:S(2)}, u32[]{:S(2)}) async-start(bf16[16,48,256]{2,1,0:T(8,128)(2,1)} %bitcast.17), calls=%async_computation.7 | async-start | bytes 786432 | tf_op jit(solution)/shard_map/all_to_all | solution.py:296
  160.8 17.7 %all-gather.2.cloned.1.call-done.kv = bf16[8192,128]{1,0:T(8,128)(2,1)} async-done(((bf16[256,128]{1,0:T(8,128)(2,1)}), bf16[8192,128]{1,0:T(8,128)(2,1)}) %all-gather.2.cloned.1.call-update) | async-done | bytes 2097168 | tf_op jit(solution)/shard_map/all_gather | solution.py:343
  178.4 1.6 copy-done.17
  180.0 5.9 %shard_map.138 = bf16[256,128]{1,0:T(8,128)(2,1)S(1)} custom-call(bf16[2,256,128]{2,1,0:T(8,128)(2,1)S(1)} %copy-done.19, bf16[8192,128]{1,0:T(8,128)(2,1)S(1)} %copy-done.17), custom_call_target="tpu_custom_call" | custom-call | flops 2306867200 | tf_op jit(solution)/shard_map/pallas_call | solution.py:272
  185.9 5.9 %shard_map.139 = bf16[256,128]{1,0:T(8,128)(2,1)S(1)} custom-call(bf16[2,256,128]{2,1,0:T(8,128)(2,1)S(1)} %get-tuple-element.29.q, bf16[8192,128]{1,0:T(8,128)(2,1)S(1)} %copy-done.17), custom_call_target="tpu_custom_call" | custom-call | flops 2306867200 | tf_op jit(solution)/shard_map/pallas_call | solution.py:272
  192.5 1.3 shard_map.140
  (54 shorter events, 8.0 us)
Async XLA Ops:
  7.2 19.8 %copy-start.9 = (bf16[256,256]{1,0:T(8,128)(2,1)S(1)}, bf16[256,256]{1,0:T(8,128)(2,1)}, u32[]{:S(2)}) copy-start(bf16[256,256]{1,0:T(8,128)(2,1)} %q.1) | copy-start | bytes 393220
  7.2 0.9 copy-start.10
  8.1 0.7 copy-start.13
  8.8 18.2 %copy-start.11 = (bf16[256,64]{0,1:T(8,128)(2,1)S(1)}, bf16[256,64]{0,1:T(8,128)(2,1)}, u32[]{:S(2)}) copy-start(bf16[256,64]{0,1:T(8,128)(2,1)} %param.13) | copy-start | bytes 98308
  8.8 18.2 %copy-start.12 = (bf16[256,64]{0,1:T(8,128)(2,1)S(1)}, bf16[256,64]{0,1:T(8,128)(2,1)}, u32[]{:S(2)}) copy-start(bf16[256,64]{0,1:T(8,128)(2,1)} %param.14) | copy-start | bytes 98308
  10.0 33.8 %all-to-all-start = ((bf16[16,48,256]{2,1,0:T(8,128)(2,1)}), bf16[16,48,256]{2,1,0:T(8,128)(2,1)S(1)}, u32[]{:S(2)}, u32[]{:S(2)}) async-start(bf16[16,48,256]{2,1,0:T(8,128)(2,1)} %bitcast.4), calls=%async_computation | async-start | bytes 786432 | tf_op jit(solution)/shard_map/all_to_all | solution.py:296
  27.9 0.7 copy-start.18
  55.5 4.4 %copy-start.6 = (bf16[1,4096,128]{2,1,0:T(8,128)(2,1)S(1)}, bf16[1,4096,128]{2,1,0:T(8,128)(2,1)}, u32[]{:S(2)}) copy-start(bf16[1,4096,128]{2,1,0:T(8,128)(2,1)} %param.21) | copy-start | bytes 3145732
  55.5 36.5 %all-to-all-start.2 = ((bf16[4,768,256]{2,1,0:T(8,128)(2,1)}), bf16[4,768,256]{2,1,0:T(8,128)(2,1)S(1)}, u32[]{:S(2)}, u32[]{:S(2)}) async-start(bf16[4,768,256]{2,1,0:T(8,128)(2,1)} %broadcast_in_dim.8), calls=%async_computation.2 | async-start | bytes 3145728 | tf_op jit(solution)/shard_map/all_to_all | solution.py:296
  59.9 1.2 copy-start.7
  61.1 1.2 copy-start.8
  63.3 18.5 %collective-permute-start = (bf16[1536,256]{1,0:T(8,128)(2,1)S(1)}, bf16[1536,256]{1,0:T(8,128)(2,1)S(1)}, u32[]{:S(2)}, u32[]{:S(2)}) collective-permute-start(bf16[1536,256]{1,0:T(8,128)(2,1)S(1)} %get-tuple-element.21), channel_id=1, source_target_pairs={{0,4},{4,8},{8,12},{12,0},{1,5},{5,9},{9,13},{13,1},{2,6},{6,10},{... | collective-permute-start | bytes 2359304 | tf_op jit(solution)/shard_map/ppermute | solution.py:291
  66.4 23.7 %collective-permute-start.1 = (bf16[1536,256]{1,0:T(8,128)(2,1)S(1)}, bf16[1536,256]{1,0:T(8,128)(2,1)S(1)}, u32[]{:S(2)}, u32[]{:S(2)}) collective-permute-start(bf16[1536,256]{1,0:T(8,128)(2,1)S(1)} %get-tuple-element.22), channel_id=1, source_target_pairs={{0,8},{4,12},{8,0},{12,4},{1,9},{5,13},{9,1},{13,5},{2,10},{6,14},... | collective-permute-start | bytes 2359304 | tf_op jit(solution)/shard_map/ppermute | solution.py:291
  70.8 20.2 %collective-permute-start.2 = (bf16[1536,256]{1,0:T(8,128)(2,1)S(1)}, bf16[1536,256]{1,0:T(8,128)(2,1)S(1)}, u32[]{:S(2)}, u32[]{:S(2)}) collective-permute-start(bf16[1536,256]{1,0:T(8,128)(2,1)S(1)} %get-tuple-element.23), channel_id=1, source_target_pairs={{0,12},{4,0},{8,4},{12,8},{1,13},{5,1},{9,5},{13,9},{2,14},{6,2},{... | collective-permute-start | bytes 2359304 | tf_op jit(solution)/shard_map/ppermute | solution.py:291
  90.2 0.9 copy-start
  91.0 0.9 copy-start.3
  92.0 1.1 copy-start.1
  93.1 1.1 copy-start.4
  98.5 17.4 %all-to-all-start.3 = ((f16[4,776,256]{2,1,0:T(8,128)(2,1)}), f16[4,776,256]{2,1,0:T(8,128)(2,1)}, u32[]{:S(2)}, u32[]{:S(2)}) async-start(f16[4,776,256]{2,1,0:T(8,128)(2,1)} %convert_element_type.14), calls=%async_computation.3 | async-start | bytes 3178496 | tf_op jit(solution)/shard_map/all_to_all | solution.py:296
  102.9 75.6 %all-gather.2.cloned.1.call-start = ((), (), s32[]{:S(2)}) async-start(), calls=%async_computation.8 | async-start | bytes 2162688 | tf_op jit(solution)/shard_map/all_gather | solution.py:343
  117.6 12.8 %copy-start.2 = (bf16[1536,256]{1,0:T(8,128)(2,1)S(1)}, bf16[1536,256]{1,0:T(8,128)(2,1)}, u32[]{:S(2)}) copy-start(bf16[1536,256]{1,0:T(8,128)(2,1)} %copy-done) | copy-start | bytes 2359300
  117.6 12.8 %copy-start.5 = (bf16[1536,256]{1,0:T(8,128)(2,1)S(1)}, bf16[1536,256]{1,0:T(8,128)(2,1)}, u32[]{:S(2)}) copy-start(bf16[1536,256]{1,0:T(8,128)(2,1)} %copy-done.3) | copy-start | bytes 2359300
  147.1 31.4 %copy-start.19 = (bf16[2,256,128]{2,1,0:T(8,128)(2,1)S(1)}, bf16[2,256,128]{2,1,0:T(8,128)(2,1)}, u32[]{:S(2)}) copy-start(bf16[2,256,128]{2,1,0:T(8,128)(2,1)} %copy-done.18) | copy-start | bytes 393220
  154.9 37.6 %all-to-all-start.7 = ((bf16[16,48,256]{2,1,0:T(8,128)(2,1)}), bf16[16,48,256]{2,1,0:T(8,128)(2,1)S(1)}, u32[]{:S(2)}, u32[]{:S(2)}) async-start(bf16[16,48,256]{2,1,0:T(8,128)(2,1)} %bitcast.17), calls=%async_computation.7 | async-start | bytes 786432 | tf_op jit(solution)/shard_map/all_to_all | solution.py:296
  178.4 1.6 copy-start.17
  185.9 6.6 %copy-start.14 = (s32[256,2]{0,1:T(2,128)S(1)}, s32[256,2]{0,1:T(2,128)}, u32[]{:S(2)}) copy-start(s32[256,2]{0,1:T(2,128)} %param.18) | copy-start | bytes 6148
  185.9 6.6 %copy-start.15 = (f32[256,2]{0,1:T(2,128)S(1)}, f32[256,2]{0,1:T(2,128)}, u32[]{:S(2)}) copy-start(f32[256,2]{0,1:T(2,128)} %param.20) | copy-start | bytes 6148
  185.9 6.6 %copy-start.16 = (f32[256]{0:T(256)S(1)}, f32[256]{0:T(256)}, u32[]{:S(2)}) copy-start(f32[256]{0:T(256)} %param.19) | copy-start | bytes 3076
Sparse Core Ops, SparseCore 0:
  106.4 72.0 all-gather.1

commit v3 on v2

--- a/solution.py
+++ b/solution.py
@@ -93,16 +93,14 @@
     return jnp.concatenate(parts, axis=0)
 
 
-def rope_fn(queries, keys_t, values_t, table):
-    q_t = queries.astype(F32).T
-    q_gain, k_gain = table[64:128], table[128:192]
-    heads = []
-    for h in range(4):
-        turned = rotated(q_t[h * HEAD_DIM : (h + 1) * HEAD_DIM], q_gain, table) * 0.125
-        heads.append(jnp.concatenate([turned, jnp.zeros_like(turned)], axis=0).T.astype(BF))
-    k = rotated(keys_t.astype(F32), k_gain, table)
-    kv = jnp.concatenate([k, values_t.astype(F32)], axis=0).T.astype(BF)
-    return heads, kv
+def query_fn(queries, table):
+    turned = rotated(queries.astype(F32).T, table[64:128], table) * 0.125
+    return jnp.concatenate([turned, jnp.zeros_like(turned)], axis=0).T.astype(BF)
+
+
+def key_fn(keys_t, values_t, table):
+    k = rotated(keys_t.astype(F32), table[128:192], table)
+    return jnp.concatenate([k, values_t.astype(F32)], axis=0).T.astype(BF)
 
 
 def gate_up_fn(get_tokens, get_weight, put):
@@ -168,12 +166,12 @@
     out[...] = combine_fn(ids[...], gw[...], ew[...], res[...])
 
 
-def rope_kernel(q, k, v, table, q_first, q_second, kv_out):
-    heads, kv = rope_fn(q[...], k[...], v[...], table[...])
-    for h in range(2):
-        q_first[h] = heads[h]
-        q_second[h] = heads[2 + h]
-    kv_out[...] = kv
+def query_kernel(q, table, out, *, head):
+    out[...] = query_fn(q[:, head * HEAD_DIM : (head + 1) * HEAD_DIM], table[...])
+
+
+def key_kernel(k, v, table, out):
+    out[...] = key_fn(k[...], v[...], table[...])
 
 
 def pack_kernel(at, gate, up, down, *outs):
@@ -226,8 +224,9 @@
 KEYS = 1024
 
 
-def attend_kernel(q, kv, out, scores):
-    blocks = [(kv, i) for i in range(kv.shape[0] // KEYS)]
+def attend_kernel(q_first, q_second, own, other, out, scores):
+    q = (q_first, q_second)
+    blocks = [(ref, i) for ref in (own, other) for i in range(ref.shape[0] // KEYS)]
 
     def lanes(v, op):
         parts = [v[:, 128 * i : 128 * (i + 1)] for i in range(v.shape[1] // 128)]
@@ -236,7 +235,7 @@
     def score(h, j):
         ref, i = blocks[j]
         s = lax.dot_general(
-            q[h], ref[i * KEYS : (i + 1) * KEYS, :], (((1,), (1,)), ((), ())), preferred_element_type=F32
+            q[h][...], ref[i * KEYS : (i + 1) * KEYS, :], (((1,), (1,)), ((), ())), preferred_element_type=F32
         )
         scores[h, :, j * KEYS : (j + 1) * KEYS] = s
         return lanes(s, jnp.maximum)
@@ -307,9 +306,23 @@
     )
 
 
-def attend(q, kv):
-    scratch = [pltpu.VMEM((2, TOK, kv.shape[0]), F32)]
-    return call(attend_kernel, array(TOK, 128), q, kv, flops=2200 << 20, scratch=scratch, vmem=36)
+def attend(q, own, other):
+    scratch = [pltpu.VMEM((2, TOK, 2 * own.shape[0]), F32)]
+    return call(attend_kernel, array(TOK, 128), *q, own, other, flops=2200 << 20, scratch=scratch, vmem=32)
+
+
+def moved(kv, shift):
+    return lax.ppermute(kv, "z", [(i, (i + shift) % 16) for i in range(16)])
+
+
+def join_kernel(a, b, out):
+    out[: a.shape[0]] = a[...]
+    out[a.shape[0] :] = b[...]
+
+
+def rotate_queries(q, table, head):
+    kernel = functools.partial(query_kernel, head=head)
+    return call(kernel, array(TOK, 128), q, table, flops=2 << 20)
 
 
 def on_device(
@@ -331,22 +344,17 @@
     routed = call(route_kernel, array(SLOTS, 256), ids, moe_rows, flops=4 << 20)
     arrived = exchange(routed.reshape(16, 2 * CAP, 256), "z")
     table = rope_table(query_gain, key_gain)
-    *q_heads, kv = call(
-        rope_kernel,
-        (array(2, TOK, 128),) * 2 + (array(TOK, 128),),
-        queries,
-        keys.T,
-        values.T,
-        table,
-        flops=4 << 20,
-    )
-    kv = lax.all_gather(kv, EP, axis=0, tiled=True)
+    kv = call(key_kernel, array(TOK, 128), keys.T, values.T, table, flops=2 << 20)
     flip = lax.axis_index("c")
     y, x = lax.axis_index("y"), lax.axis_index("x")
     at = jnp.stack([y + flip * (x - y), 4 - 3 * flip, 1 + 3 * flip]).astype(jnp.int32)
     packed = call(pack_kernel, (array(1536, 256),) * 4, at, expert_gate[0], expert_up[0], expert_down[0])
     weights = shifted(packed)
-    arrived, q_heads = tie((arrived, q_heads))
+    arrived, kv, table = tie((arrived, kv, table))
+    for shift in (8, 4, -2):
+        kv = jnp.concatenate([kv, moved(kv, shift)], axis=0)
+    last = moved(kv, 1)
+    q_heads = [rotate_queries(queries, table, head) for head in range(4)]
     rows = arrived.reshape(16, 2, CAP, 256).transpose(1, 0, 2, 3).reshape(2, HALF, 256)
     rows = exchange(rows, "c").reshape(1, SLOTS, 256)
     tokens = exchange(jnp.broadcast_to(rows, (4, SLOTS, 256)), ACROSS, GATHER)
@@ -363,9 +371,11 @@
     reduced = call(reduce_kernel, array(2, HALF, 256), summands, flops=4 << 20)
     reduced = exchange(reduced, "c")
     reduced = reduced.reshape(2, 16, CAP, 256).transpose(1, 0, 2, 3).reshape(16, 2 * CAP, 256)
-    reduced, q_heads = tie((reduced, q_heads))
+    reduced, q_heads, kv = tie((reduced, q_heads, kv))
     returned = exchange(reduced, "z")
-    attended = jnp.concatenate([attend(q, kv) for q in q_heads], axis=1)
+    kv = call(join_kernel, array(16 * TOK, 128), kv, last)
+    other = lax.ppermute(kv, "c", [(0, 1), (1, 0)])
+    attended = jnp.concatenate([attend(q_heads[i : i + 2], kv, other) for i in (0, 2)], axis=1)
     returned, attended = tie((returned, attended))
     moe_out = call(
         combine_kernel,

time: 202 us -> 213 us (1.054)
  the two profiles are of different devices: /device:TPU:1 before, /device:TPU:24 now
where the time goes in v3:
time: 213 us; the launch traced here: 212 us
  waiting for transfers between devices  77 us (36%)
  starting transfers between devices  68.2 us (32%)
  blocking collectives  24.7 us (12%)
  Pallas kernels  23.5 us (11%)
  local copies, waits for them, and re-layouts  13.6 us (6%)
  other arithmetic  3.87 us (2%)
    all_to_all x5, starting transfers between devices, exchange(): lax.all_to_all(a, axes, split_axis=0, concat_axis=0, axis_index_groups=gr...  35.8 us
    all_to_all x5, waiting for transfers between devices, exchange(): lax.all_to_all(a, axes, split_axis=0, concat_axis=0, axis_index_groups=gr...  34.9 us
    ppermute x4, waiting for transfers between devices, moved(): return lax.ppermute(kv, 'z', [(i, (i + shift) % 16) for i in range(16)])  25.6 us
    all_to_all x3, blocking collectives, exchange(): lax.all_to_all(a, axes, split_axis=0, concat_axis=0, axis_index_groups=gr...  24.7 us
    pallas_call x15, Pallas kernels, call(): pl.pallas_call(kernel, out_shape=outs, in_specs=[spec(a) for a in args],...  23.5 us
    ppermute x4, starting transfers between devices, moved(): return lax.ppermute(kv, 'z', [(i, (i + shift) % 16) for i in range(16)])  21.9 us
    ppermute x3, waiting for transfers between devices, shifted(): out.append(lax.ppermute(blocks[s], ACROSS, pairs))  16.5 us
    unnamed x37, local copies, waits for them, and re-layouts  11.4 us
  transfers between devices with their start and end apart: 13, of which 8 were waited for; matrix products, arithmetic and copies ran while one was open for 2% of the time, Pallas kernels for 8%

profile of v3, /device:TPU:24, one launch (start us, length us, event | category | flops | bytes accessed | tf_op | source)
XLA Modules:
  0.0 211.9 jit_solution(16215726449155992453)
XLA Ops:
  3.4 15.2 %all-to-all-start = ((bf16[16,48,256]{2,1,0:T(8,128)(2,1)}), bf16[16,48,256]{2,1,0:T(8,128)(2,1)S(1)}, u32[]{:S(2)}, u32[]{:S(2)}) async-start(bf16[16,48,256]{2,1,0:T(8,128)(2,1)} %bitcast.4), calls=%async_computation | async-start | bytes 786432 | tf_op jit(solution)/shard_map/all_to_all | solution.py:295
  20.0 22.5 %all-to-all-done = bf16[16,48,256]{2,1,0:T(8,128)(2,1)S(1)} async-done(((bf16[16,48,256]{2,1,0:T(8,128)(2,1)}), bf16[16,48,256]{2,1,0:T(8,128)(2,1)S(1)}, u32[]{:S(2)}, u32[]{:S(2)}) %all-to-all-start) | async-done | bytes 393248 | tf_op jit(solution)/shard_map/all_to_all | solution.py:295
  42.5 4.0 %all_to_all.40 = bf16[2,384,256]{2,1,0:T(8,128)(2,1)S(1)} all-to-all(bf16[2,384,256]{2,1,0:T(8,128)(2,1)S(1)} %bitcast.40), channel_id=1, replica_groups=mesh['z'=16,'c'=2,'y'=4,'x'=4] {'c'}, dimensions={0} | all-to-all | bytes 786432 | tf_op jit(solution)/shard_map/all_to_all | solution.py:295
  46.5 1.3 broadcast_in_dim.8
  47.8 4.3 %all-to-all-start.2 = ((bf16[4,768,256]{2,1,0:T(8,128)(2,1)}), bf16[4,768,256]{2,1,0:T(8,128)(2,1)S(1)}, u32[]{:S(2)}, u32[]{:S(2)}) async-start(bf16[4,768,256]{2,1,0:T(8,128)(2,1)} %broadcast_in_dim.8), calls=%async_computation.2 | async-start | bytes 3145728 | tf_op jit(solution)/shard_map/all_to_all | solution.py:295
  52.1 1.2 copy-done.7
  53.4 1.2 copy-done.8
  56.8 2.1 %collective-permute-start = (bf16[1536,256]{1,0:T(8,128)(2,1)S(1)}, bf16[1536,256]{1,0:T(8,128)(2,1)S(1)}, u32[]{:S(2)}, u32[]{:S(2)}) collective-permute-start(bf16[1536,256]{1,0:T(8,128)(2,1)S(1)} %get-tuple-element.19), channel_id=1, source_target_pairs={{0,4},{4,8},{8,12},{12,0},{1,5},{5,9},{9,13},{13,1},{2,6},{6,10},{... | collective-permute-start | bytes 2359304 | tf_op jit(solution)/shard_map/ppermute | solution.py:290
  58.9 4.5 %collective-permute-start.1 = (bf16[1536,256]{1,0:T(8,128)(2,1)S(1)}, bf16[1536,256]{1,0:T(8,128)(2,1)S(1)}, u32[]{:S(2)}, u32[]{:S(2)}) collective-permute-start(bf16[1536,256]{1,0:T(8,128)(2,1)S(1)} %get-tuple-element.20), channel_id=1, source_target_pairs={{0,8},{4,12},{8,0},{12,4},{1,9},{5,13},{9,1},{13,5},{2,10},{6,14},... | collective-permute-start | bytes 2359304 | tf_op jit(solution)/shard_map/ppermute | solution.py:290
  63.4 1.9 collective-permute-start.2
  65.4 5.4 %collective-permute-done.w1 = bf16[1536,256]{1,0:T(8,128)(2,1)S(1)} collective-permute-done((bf16[1536,256]{1,0:T(8,128)(2,1)S(1)}, bf16[1536,256]{1,0:T(8,128)(2,1)S(1)}, u32[]{:S(2)}, u32[]{:S(2)}) %collective-permute-start) | collective-permute-done | bytes 786464 | tf_op jit(solution)/shard_map/ppermute | solution.py:290
  70.8 3.6 %collective-permute-done.1.w2 = bf16[1536,256]{1,0:T(8,128)(2,1)S(1)} collective-permute-done((bf16[1536,256]{1,0:T(8,128)(2,1)S(1)}, bf16[1536,256]{1,0:T(8,128)(2,1)S(1)}, u32[]{:S(2)}, u32[]{:S(2)}) %collective-permute-start.1) | collective-permute-done | bytes 786464 | tf_op jit(solution)/shard_map/ppermute | solution.py:290
  75.3 7.4 %collective-permute-done.2.w3 = bf16[1536,256]{1,0:T(8,128)(2,1)S(1)} collective-permute-done((bf16[1536,256]{1,0:T(8,128)(2,1)S(1)}, bf16[1536,256]{1,0:T(8,128)(2,1)S(1)}, u32[]{:S(2)}, u32[]{:S(2)}) %collective-permute-start.2) | collective-permute-done | bytes 786464 | tf_op jit(solution)/shard_map/ppermute | solution.py:290
  85.9 2.8 %shard_map.134 = f32[4,776,256]{2,1,0:T(8,128)S(1)} custom-call(s32[3]{0:T(128)S(1)} %pad_add_fusion.at, bf16[4,768,256]{2,1,0:T(8,128)(2,1)S(1)} %all-to-all-done.2.tokens, bf16[1536,256]{1,0:T(8,128)(2,1)S(1)} %get-tuple-element.18.w0, bf16[1536,256]{1,0:T(8,128)(2,1)S(1)} %collective-permute-done.w1, bf16[1536,256]{1,0:T(8,128)(2,1)S(1)} %copy-done.1, ...), custom_call_target="tpu_custom_call" | custom-call | flops 1677721600 | tf_op jit(solution)/shard_map/pallas_call | solution.py:271
  89.0 16.6 %all_to_all.41 = f16[4,776,256]{2,1,0:T(8,128)(2,1)S(1)} all-to-all(f16[4,776,256]{2,1,0:T(8,128)(2,1)S(1)} %convert_element_type.14), channel_id=1, replica_groups={{0,4,8,12},{1,5,9,13},{2,6,10,14},{3,7,11,15},{16,17,18,19},{20,21,22,2..., dimensions={0} | all-to-all | bytes 3178496 | tf_op jit(solution)/shard_map/all_to_all | solution.py:295
  107.0 4.8 %all-to-all-start.4 = ((bf16[4,768,128]{2,1,0:T(8,128)(2,1)}), bf16[4,768,128]{2,1,0:T(8,128)(2,1)S(1)}, u32[]{:S(2)}, u32[]{:S(2)}) async-start(bf16[4,768,128]{2,1,0:T(8,128)(2,1)} %shard_map.135), calls=%async_computation.4 | async-start | bytes 1572864 | tf_op jit(solution)/shard_map/all_to_all | solution.py:295
  111.8 6.5 %collective-permute-start.3 = (bf16[256,128]{1,0:T(8,128)(2,1)S(1)}, bf16[256,128]{1,0:T(8,128)(2,1)S(1)}, u32[]{:S(2)}, u32[]{:S(2)}) collective-permute-start(bf16[256,128]{1,0:T(8,128)(2,1)S(1)} %shard_map.132), channel_id=1, source_target_pairs={{0,256},{32,288},{64,320},{96,352},{128,384},{160,416},{192,448},{... | collective-permute-start | bytes 196616 | tf_op jit(solution)/shard_map/ppermute | solution.py:315
  118.3 8.4 %collective-permute-done.3 = bf16[256,128]{1,0:T(8,128)(2,1)S(1)} collective-permute-done((bf16[256,128]{1,0:T(8,128)(2,1)S(1)}, bf16[256,128]{1,0:T(8,128)(2,1)S(1)}, u32[]{:S(2)}, u32[]{:S(2)}) %collective-permute-start.3) | collective-permute-done | bytes 65568 | tf_op jit(solution)/shard_map/ppermute | solution.py:315
  127.4 5.7 %collective-permute-start.4 = (bf16[512,128]{1,0:T(8,128)(2,1)}, bf16[512,128]{1,0:T(8,128)(2,1)}, u32[]{:S(2)}, u32[]{:S(2)}) collective-permute-start(bf16[512,128]{1,0:T(8,128)(2,1)} %pad_maximum_fusion.1), channel_id=1, source_target_pairs={{0,128},{32,160},{64,192},{96,224},{128,256},{160,288},{192,320},{... | collective-permute-start | bytes 393224 | tf_op jit(solution)/shard_map/ppermute | solution.py:315
  134.2 2.7 %shard_map.136 = bf16[4,768,256]{2,1,0:T(8,128)(2,1)} custom-call(s32[3]{0:T(128)S(1)} %pad_add_fusion.at, bf16[4,768,128]{2,1,0:T(8,128)(2,1)S(1)} %all-to-all-done.4.hidden, bf16[1536,256]{1,0:T(8,128)(2,1)S(1)} %get-tuple-element.18.w0, bf16[1536,256]{1,0:T(8,128)(2,1)S(1)} %collective-permute-done.w1, bf16[1536,256]{1,0:T(8,128)(2,1)S(1)} %copy-done.2, ...), custom_call_target="tpu_custom_call" | custom-call | flops 838860800 | tf_op jit(solution)/shard_map/pallas_call | solution.py:271
  137.0 5.9 %all-to-all-start.5 = ((bf16[4,768,256]{2,1,0:T(8,128)(2,1)}), bf16[4,768,256]{2,1,0:T(8,128)(2,1)S(1)}, u32[]{:S(2)}, u32[]{:S(2)}) async-start(bf16[4,768,256]{2,1,0:T(8,128)(2,1)} %shard_map.136), calls=%async_computation.5 | async-start | bytes 3145728 | tf_op jit(solution)/shard_map/all_to_all | solution.py:295
  143.8 7.8 %collective-permute-start.5 = (bf16[1024,128]{1,0:T(8,128)(2,1)S(1)}, bf16[1024,128]{1,0:T(8,128)(2,1)S(1)}, u32[]{:S(2)}, u32[]{:S(2)}) collective-permute-start(bf16[1024,128]{1,0:T(8,128)(2,1)S(1)} %pad_maximum_fusion), channel_id=1, source_target_pairs={{0,448},{32,480},{64,0},{96,32},{128,64},{160,96},{192,128},{224,1... | collective-permute-start | bytes 786440 | tf_op jit(solution)/shard_map/ppermute | solution.py:315
  152.6 9.1 %collective-permute-done.5 = bf16[1024,128]{1,0:T(8,128)(2,1)S(1)} collective-permute-done((bf16[1024,128]{1,0:T(8,128)(2,1)S(1)}, bf16[1024,128]{1,0:T(8,128)(2,1)S(1)}, u32[]{:S(2)}, u32[]{:S(2)}) %collective-permute-start.5) | collective-permute-done | bytes 262176 | tf_op jit(solution)/shard_map/ppermute | solution.py:315
  161.7 1.9 collective-permute-start.6
  164.9 4.0 %all_to_all.42 = bf16[2,384,256]{2,1,0:T(8,128)(2,1)S(1)} all-to-all(bf16[2,384,256]{2,1,0:T(8,128)(2,1)S(1)} %shard_map.137), channel_id=1, replica_groups=mesh['z'=16,'c'=2,'y'=4,'x'=4] {'c'}, dimensions={0} | all-to-all | bytes 786432 | tf_op jit(solution)/shard_map/all_to_all | solution.py:295
  169.7 8.0 %collective-permute-done.6.b = bf16[2048,128]{1,0:T(8,128)(2,1)S(1)} collective-permute-done((bf16[2048,128]{1,0:T(8,128)(2,1)S(1)}, bf16[2048,128]{1,0:T(8,128)(2,1)S(1)}, u32[]{:S(2)}, u32[]{:S(2)}) %collective-permute-start.6) | collective-permute-done | bytes 524320 | tf_op jit(solution)/shard_map/ppermute | solution.py:315
  177.8 1.9 collective-permute-start.7
  179.7 5.6 %all-to-all-start.7 = ((bf16[16,48,256]{2,1,0:T(8,128)(2,1)}), bf16[16,48,256]{2,1,0:T(8,128)(2,1)S(1)}, u32[]{:S(2)}, u32[]{:S(2)}) async-start(bf16[16,48,256]{2,1,0:T(8,128)(2,1)} %bitcast.39), calls=%async_computation.7 | async-start | bytes 786432 | tf_op jit(solution)/shard_map/all_to_all | solution.py:295
  185.3 6.0 %shard_map.143 = bf16[256,128]{1,0:T(8,128)(2,1)S(1)} custom-call(bf16[256,128]{1,0:T(8,128)(2,1)S(1)} %shard_map.138.q_first, bf16[256,128]{1,0:T(8,128)(2,1)S(1)} %shard_map.139.q_second, bf16[4096,128]{1,0:T(8,128)(2,1)S(1)} %shard_map.142.own, bf16[4096,128]{1,0:T(8,128)(2,1)S(1)} %collective-permute-done.7.other), custom_call_target="tpu_custom_call" | custom-call | flops 2306867200 | tf_op jit(solution)/shard_map/pallas_call | solution.py:271
  191.4 6.0 %shard_map.144 = bf16[256,128]{1,0:T(8,128)(2,1)S(1)} custom-call(bf16[256,128]{1,0:T(8,128)(2,1)S(1)} %shard_map.140.q_first, bf16[256,128]{1,0:T(8,128)(2,1)S(1)} %shard_map.141.q_second, bf16[4096,128]{1,0:T(8,128)(2,1)S(1)} %shard_map.142.own, bf16[4096,128]{1,0:T(8,128)(2,1)S(1)} %collective-permute-done.7.other), custom_call_target="tpu_custom_call" | custom-call | flops 2306867200 | tf_op jit(solution)/shard_map/pallas_call | solution.py:271
  198.0 12.5 %all-to-all-done.7 = bf16[16,48,256]{2,1,0:T(8,128)(2,1)S(1)} async-done(((bf16[16,48,256]{2,1,0:T(8,128)(2,1)}), bf16[16,48,256]{2,1,0:T(8,128)(2,1)S(1)}, u32[]{:S(2)}, u32[]{:S(2)}) %all-to-all-start.7) | async-done | bytes 393248 | tf_op jit(solution)/shard_map/all_to_all | solution.py:295
  210.5 1.3 shard_map.145
  (67 shorter events, 18.5 us)
Async XLA Ops:
  0.6 0.9 copy-start.10
  1.5 0.7 copy-start.13
  2.2 17.6 %copy-start.11 = (bf16[256,64]{0,1:T(8,128)(2,1)S(1)}, bf16[256,64]{0,1:T(8,128)(2,1)}, u32[]{:S(2)}) copy-start(bf16[256,64]{0,1:T(8,128)(2,1)} %param.13) | copy-start | bytes 98308
  2.2 17.6 %copy-start.12 = (bf16[256,64]{0,1:T(8,128)(2,1)S(1)}, bf16[256,64]{0,1:T(8,128)(2,1)}, u32[]{:S(2)}) copy-start(bf16[256,64]{0,1:T(8,128)(2,1)} %param.14) | copy-start | bytes 98308
  3.4 39.0 %all-to-all-start = ((bf16[16,48,256]{2,1,0:T(8,128)(2,1)}), bf16[16,48,256]{2,1,0:T(8,128)(2,1)S(1)}, u32[]{:S(2)}, u32[]{:S(2)}) async-start(bf16[16,48,256]{2,1,0:T(8,128)(2,1)} %bitcast.4), calls=%async_computation | async-start | bytes 786432 | tf_op jit(solution)/shard_map/all_to_all | solution.py:295
  47.8 35.9 %all-to-all-start.2 = ((bf16[4,768,256]{2,1,0:T(8,128)(2,1)}), bf16[4,768,256]{2,1,0:T(8,128)(2,1)S(1)}, u32[]{:S(2)}, u32[]{:S(2)}) async-start(bf16[4,768,256]{2,1,0:T(8,128)(2,1)} %broadcast_in_dim.8), calls=%async_computation.2 | async-start | bytes 3145728 | tf_op jit(solution)/shard_map/all_to_all | solution.py:295
  52.1 1.2 copy-start.7
  53.4 1.2 copy-start.8
  54.6 1.2 copy-start.9
  56.8 14.0 %collective-permute-start = (bf16[1536,256]{1,0:T(8,128)(2,1)S(1)}, bf16[1536,256]{1,0:T(8,128)(2,1)S(1)}, u32[]{:S(2)}, u32[]{:S(2)}) collective-permute-start(bf16[1536,256]{1,0:T(8,128)(2,1)S(1)} %get-tuple-element.19), channel_id=1, source_target_pairs={{0,4},{4,8},{8,12},{12,0},{1,5},{5,9},{9,13},{13,1},{2,6},{6,10},{... | collective-permute-start | bytes 2359304 | tf_op jit(solution)/shard_map/ppermute | solution.py:290
  58.9 15.5 %collective-permute-start.1 = (bf16[1536,256]{1,0:T(8,128)(2,1)S(1)}, bf16[1536,256]{1,0:T(8,128)(2,1)S(1)}, u32[]{:S(2)}, u32[]{:S(2)}) collective-permute-start(bf16[1536,256]{1,0:T(8,128)(2,1)S(1)} %get-tuple-element.20), channel_id=1, source_target_pairs={{0,8},{4,12},{8,0},{12,4},{1,9},{5,13},{9,1},{13,5},{2,10},{6,14},... | collective-permute-start | bytes 2359304 | tf_op jit(solution)/shard_map/ppermute | solution.py:290
  63.4 19.3 %collective-permute-start.2 = (bf16[1536,256]{1,0:T(8,128)(2,1)S(1)}, bf16[1536,256]{1,0:T(8,128)(2,1)S(1)}, u32[]{:S(2)}, u32[]{:S(2)}) collective-permute-start(bf16[1536,256]{1,0:T(8,128)(2,1)S(1)} %get-tuple-element.21), channel_id=1, source_target_pairs={{0,12},{4,0},{8,4},{12,8},{1,13},{5,1},{9,5},{13,9},{2,14},{6,2},{... | collective-permute-start | bytes 2359304 | tf_op jit(solution)/shard_map/ppermute | solution.py:290
  74.4 0.9 copy-start
  82.7 0.9 copy-start.3
  83.7 1.1 copy-start.1
  84.8 1.1 copy-start.4
  105.8 27.3 %copy-start.2 = (bf16[1536,256]{1,0:T(8,128)(2,1)S(1)}, bf16[1536,256]{1,0:T(8,128)(2,1)}, u32[]{:S(2)}) copy-start(bf16[1536,256]{1,0:T(8,128)(2,1)} %copy-done) | copy-start | bytes 2359300
  107.0 26.1 %all-to-all-start.4 = ((bf16[4,768,128]{2,1,0:T(8,128)(2,1)}), bf16[4,768,128]{2,1,0:T(8,128)(2,1)S(1)}, u32[]{:S(2)}, u32[]{:S(2)}) async-start(bf16[4,768,128]{2,1,0:T(8,128)(2,1)} %shard_map.135), calls=%async_computation.4 | async-start | bytes 1572864 | tf_op jit(solution)/shard_map/all_to_all | solution.py:295
  111.8 14.9 %collective-permute-start.3 = (bf16[256,128]{1,0:T(8,128)(2,1)S(1)}, bf16[256,128]{1,0:T(8,128)(2,1)S(1)}, u32[]{:S(2)}, u32[]{:S(2)}) collective-permute-start(bf16[256,128]{1,0:T(8,128)(2,1)S(1)} %shard_map.132), channel_id=1, source_target_pairs={{0,256},{32,288},{64,320},{96,352},{128,384},{160,416},{192,448},{... | collective-permute-start | bytes 196616 | tf_op jit(solution)/shard_map/ppermute | solution.py:315
  127.4 15.5 %collective-permute-start.4 = (bf16[512,128]{1,0:T(8,128)(2,1)}, bf16[512,128]{1,0:T(8,128)(2,1)}, u32[]{:S(2)}, u32[]{:S(2)}) collective-permute-start(bf16[512,128]{1,0:T(8,128)(2,1)} %pad_maximum_fusion.1), channel_id=1, source_target_pairs={{0,128},{32,160},{64,192},{96,224},{128,256},{160,288},{192,320},{... | collective-permute-start | bytes 393224 | tf_op jit(solution)/shard_map/ppermute | solution.py:315
  133.1 1.1 copy-start.5
  136.9 26.7 %copy-start.6 = (bf16[256,256]{1,0:T(8,128)(2,1)S(1)}, bf16[256,256]{1,0:T(8,128)(2,1)}, u32[]{:S(2)}) copy-start(bf16[256,256]{1,0:T(8,128)(2,1)} %q.7) | copy-start | bytes 393220
  137.0 27.7 %all-to-all-start.5 = ((bf16[4,768,256]{2,1,0:T(8,128)(2,1)}), bf16[4,768,256]{2,1,0:T(8,128)(2,1)S(1)}, u32[]{:S(2)}, u32[]{:S(2)}) async-start(bf16[4,768,256]{2,1,0:T(8,128)(2,1)} %shard_map.136), calls=%async_computation.5 | async-start | bytes 3145728 | tf_op jit(solution)/shard_map/all_to_all | solution.py:295
  143.8 17.9 %collective-permute-start.5 = (bf16[1024,128]{1,0:T(8,128)(2,1)S(1)}, bf16[1024,128]{1,0:T(8,128)(2,1)S(1)}, u32[]{:S(2)}, u32[]{:S(2)}) collective-permute-start(bf16[1024,128]{1,0:T(8,128)(2,1)S(1)} %pad_maximum_fusion), channel_id=1, source_target_pairs={{0,448},{32,480},{64,0},{96,32},{128,64},{160,96},{192,128},{224,1... | collective-permute-start | bytes 786440 | tf_op jit(solution)/shard_map/ppermute | solution.py:315
  161.7 16.0 %collective-permute-start.6 = (bf16[2048,128]{1,0:T(8,128)(2,1)S(1)}, bf16[2048,128]{1,0:T(8,128)(2,1)S(1)}, u32[]{:S(2)}, u32[]{:S(2)}) collective-permute-start(bf16[2048,128]{1,0:T(8,128)(2,1)S(1)} %constant_dynamic-update-slice_fusion.a), channel_id=1, source_target_pairs={{0,32},{32,64},{64,96},{96,128},{128,160},{160,192},{192,224},{224... | collective-permute-start | bytes 1572872 | tf_op jit(solution)/shard_map/ppermute | solution.py:315
  177.8 7.6 %collective-permute-start.7 = (bf16[4096,128]{1,0:T(8,128)(2,1)S(1)}, bf16[4096,128]{1,0:T(8,128)(2,1)S(1)}, u32[]{:S(2)}, u32[]{:S(2)}) collective-permute-start(bf16[4096,128]{1,0:T(8,128)(2,1)S(1)} %shard_map.142.own), channel_id=1, source_target_pairs={{0,16},{16,0},{1,17},{17,1},{2,18},{18,2},{3,19},{19,3},{4,20},{20... | collective-permute-start | bytes 3145736 | tf_op jit(solution)/shard_map/ppermute | solution.py:377
  179.7 30.8 %all-to-all-start.7 = ((bf16[16,48,256]{2,1,0:T(8,128)(2,1)}), bf16[16,48,256]{2,1,0:T(8,128)(2,1)S(1)}, u32[]{:S(2)}, u32[]{:S(2)}) async-start(bf16[16,48,256]{2,1,0:T(8,128)(2,1)} %bitcast.39), calls=%async_computation.7 | async-start | bytes 786432 | tf_op jit(solution)/shard_map/all_to_all | solution.py:295
  191.3 19.2 %copy-start.14 = (s32[256,2]{0,1:T(2,128)S(1)}, s32[256,2]{0,1:T(2,128)}, u32[]{:S(2)}) copy-start(s32[256,2]{0,1:T(2,128)} %param.18) | copy-start | bytes 6148
  191.3 19.2 %copy-start.15 = (f32[256,2]{0,1:T(2,128)S(1)}, f32[256,2]{0,1:T(2,128)}, u32[]{:S(2)}) copy-start(f32[256,2]{0,1:T(2,128)} %param.20) | copy-start | bytes 6148
  191.4 19.2 %copy-start.16 = (f32[256]{0:T(256)S(1)}, f32[256]{0:T(256)}, u32[]{:S(2)}) copy-start(f32[256]{0:T(256)} %param.19) | copy-start | bytes 3076

commit v4 on v3

--- a/solution.py
+++ b/solution.py
@@ -224,8 +224,8 @@
 KEYS = 1024
 
 
-def attend_kernel(q_first, q_second, own, other, out, scores):
-    q = (q_first, q_second)
+def attend_kernel(q0, q1, q2, q3, own, other, out, scores):
+    q = (q0, q1, q2, q3)
     blocks = [(ref, i) for ref in (own, other) for i in range(ref.shape[0] // KEYS)]
 
     def lanes(v, op):
@@ -237,31 +237,34 @@
         s = lax.dot_general(
             q[h][...], ref[i * KEYS : (i + 1) * KEYS, :], (((1,), (1,)), ((), ())), preferred_element_type=F32
         )
-        scores[h, :, j * KEYS : (j + 1) * KEYS] = s
+        scores[h % 2, :, j * KEYS : (j + 1) * KEYS] = s
         return lanes(s, jnp.maximum)
 
     def weigh(h, j, top):
         ref, i = blocks[j]
-        p = jnp.exp(scores[h, :, j * KEYS : (j + 1) * KEYS] - top)
+        p = jnp.exp(scores[h % 2, :, j * KEYS : (j + 1) * KEYS] - top)
         return lanes(p, jnp.add), mm(p.astype(BF), ref[i * KEYS : (i + 1) * KEYS, :])
 
     n = len(blocks)
     top = functools.reduce(jnp.maximum, [score(0, j) for j in range(n)])
-    results = []
-    for h in range(2):
+    even = None
+    for h in range(len(q)):
         top = jnp.max(top, axis=1, keepdims=True)
         following = total = summed = None
         for j in range(n):
-            if h == 0:
-                m = score(1, j)
+            if h + 1 < len(q):
+                m = score(h + 1, j)
                 following = m if following is None else jnp.maximum(following, m)
             t, o = weigh(h, j, top)
             total = t if total is None else total + t
             summed = o if summed is None else summed + o
         top = following
-        results.append(summed / jnp.sum(total, axis=1, keepdims=True))
-    first = pltpu.roll(results[0], HEAD_DIM, axis=1)
-    out[...] = jnp.where(iota(first.shape, 1) < HEAD_DIM, first, results[1]).astype(BF)
+        result = summed / jnp.sum(total, axis=1, keepdims=True)
+        if h % 2 == 0:
+            even = pltpu.roll(result, HEAD_DIM, axis=1)
+        else:
+            pair = jnp.where(iota(result.shape, 1) < HEAD_DIM, even, result)
+            out[:, HEAD_DIM * (h - 1) : HEAD_DIM * (h + 1)] = pair.astype(BF)
 
 
 def call(kernel, outs, *args, flops=0, scratch=(), vmem=20, space=pltpu.VMEM):
@@ -308,7 +311,7 @@
 
 def attend(q, own, other):
     scratch = [pltpu.VMEM((2, TOK, 2 * own.shape[0]), F32)]
-    return call(attend_kernel, array(TOK, 128), *q, own, other, flops=2200 << 20, scratch=scratch, vmem=32)
+    return call(attend_kernel, array(TOK, 256), *q, own, other, flops=4400 << 20, scratch=scratch, vmem=32)
 
 
 def moved(kv, shift):
@@ -375,7 +378,7 @@
     returned = exchange(reduced, "z")
     kv = call(join_kernel, array(16 * TOK, 128), kv, last)
     other = lax.ppermute(kv, "c", [(0, 1), (1, 0)])
-    attended = jnp.concatenate([attend(q_heads[i : i + 2], kv, other) for i in (0, 2)], axis=1)
+    attended = attend(q_heads, kv, other)
     returned, attended = tie((returned, attended))
     moe_out = call(
         combine_kernel,

time: 213 us -> 213 us (level)
    pallas_call x15 -> x14, Pallas kernels: 23.5 us -> 23.2 us  [call(): pl.pallas_call(kernel, out_shape=outs, in_specs=[spec(a) for a in args],...]
where the time goes in v4:
time: 213 us; the launch traced here: 212 us
  waiting for transfers between devices  78.2 us (37%)
  starting transfers between devices  68 us (32%)
  blocking collectives  24.7 us (12%)
  Pallas kernels  23.2 us (11%)
  local copies, waits for them, and re-layouts  13.6 us (6%)
  other arithmetic  3.2 us (2%)
    all_to_all x5, waiting for transfers between devices, exchange(): lax.all_to_all(a, axes, split_axis=0, concat_axis=0, axis_index_groups=gr...  36.1 us
    all_to_all x5, starting transfers between devices, exchange(): lax.all_to_all(a, axes, split_axis=0, concat_axis=0, axis_index_groups=gr...  35.6 us
    ppermute x4, waiting for transfers between devices, moved(): return lax.ppermute(kv, 'z', [(i, (i + shift) % 16) for i in range(16)])  25.6 us
    all_to_all x3, blocking collectives, exchange(): lax.all_to_all(a, axes, split_axis=0, concat_axis=0, axis_index_groups=gr...  24.7 us
    pallas_call x14, Pallas kernels, call(): pl.pallas_call(kernel, out_shape=outs, in_specs=[spec(a) for a in args],...  23.2 us
    ppermute x4, starting transfers between devices, moved(): return lax.ppermute(kv, 'z', [(i, (i + shift) % 16) for i in range(16)])  21.9 us
    ppermute x3, waiting for transfers between devices, shifted(): out.append(lax.ppermute(blocks[s], ACROSS, pairs))  16.5 us
    unnamed x37, local copies, waits for them, and re-layouts  11.4 us
  transfers between devices with their start and end apart: 13, of which 8 were waited for; matrix products, arithmetic and copies ran while one was open for 2% of the time, Pallas kernels for 8%

profile of v4, /device:TPU:24, one launch (start us, length us, event | category | flops | bytes accessed | tf_op | source)
XLA Modules:
  0.0 211.9 jit_solution(14229847077959191369)
XLA Ops:
  3.4 15.2 %all-to-all-start = ((bf16[16,48,256]{2,1,0:T(8,128)(2,1)}), bf16[16,48,256]{2,1,0:T(8,128)(2,1)S(1)}, u32[]{:S(2)}, u32[]{:S(2)}) async-start(bf16[16,48,256]{2,1,0:T(8,128)(2,1)} %bitcast.4), calls=%async_computation | async-start | bytes 786432 | tf_op jit(solution)/shard_map/all_to_all | solution.py:298
  20.0 22.5 %all-to-all-done = bf16[16,48,256]{2,1,0:T(8,128)(2,1)S(1)} async-done(((bf16[16,48,256]{2,1,0:T(8,128)(2,1)}), bf16[16,48,256]{2,1,0:T(8,128)(2,1)S(1)}, u32[]{:S(2)}, u32[]{:S(2)}) %all-to-all-start) | async-done | bytes 393248 | tf_op jit(solution)/shard_map/all_to_all | solution.py:298
  42.5 4.0 %all_to_all.40 = bf16[2,384,256]{2,1,0:T(8,128)(2,1)S(1)} all-to-all(bf16[2,384,256]{2,1,0:T(8,128)(2,1)S(1)} %bitcast.40), channel_id=1, replica_groups=mesh['z'=16,'c'=2,'y'=4,'x'=4] {'c'}, dimensions={0} | all-to-all | bytes 786432 | tf_op jit(solution)/shard_map/all_to_all | solution.py:298
  46.5 1.3 broadcast_in_dim.8
  47.8 4.3 %all-to-all-start.2 = ((bf16[4,768,256]{2,1,0:T(8,128)(2,1)}), bf16[4,768,256]{2,1,0:T(8,128)(2,1)S(1)}, u32[]{:S(2)}, u32[]{:S(2)}) async-start(bf16[4,768,256]{2,1,0:T(8,128)(2,1)} %broadcast_in_dim.8), calls=%async_computation.2 | async-start | bytes 3145728 | tf_op jit(solution)/shard_map/all_to_all | solution.py:298
  52.1 1.2 copy-done.7
  53.4 1.2 copy-done.8
  54.6 1.2 copy-done.9
  56.8 2.1 %collective-permute-start = (bf16[1536,256]{1,0:T(8,128)(2,1)S(1)}, bf16[1536,256]{1,0:T(8,128)(2,1)S(1)}, u32[]{:S(2)}, u32[]{:S(2)}) collective-permute-start(bf16[1536,256]{1,0:T(8,128)(2,1)S(1)} %get-tuple-element.19), channel_id=1, source_target_pairs={{0,4},{4,8},{8,12},{12,0},{1,5},{5,9},{9,13},{13,1},{2,6},{6,10},{... | collective-permute-start | bytes 2359304 | tf_op jit(solution)/shard_map/ppermute | solution.py:293
  58.9 4.5 %collective-permute-start.1 = (bf16[1536,256]{1,0:T(8,128)(2,1)S(1)}, bf16[1536,256]{1,0:T(8,128)(2,1)S(1)}, u32[]{:S(2)}, u32[]{:S(2)}) collective-permute-start(bf16[1536,256]{1,0:T(8,128)(2,1)S(1)} %get-tuple-element.20), channel_id=1, source_target_pairs={{0,8},{4,12},{8,0},{12,4},{1,9},{5,13},{9,1},{13,5},{2,10},{6,14},... | collective-permute-start | bytes 2359304 | tf_op jit(solution)/shard_map/ppermute | solution.py:293
  63.4 1.9 collective-permute-start.2
  65.4 5.4 %collective-permute-done.w1 = bf16[1536,256]{1,0:T(8,128)(2,1)S(1)} collective-permute-done((bf16[1536,256]{1,0:T(8,128)(2,1)S(1)}, bf16[1536,256]{1,0:T(8,128)(2,1)S(1)}, u32[]{:S(2)}, u32[]{:S(2)}) %collective-permute-start) | collective-permute-done | bytes 786464 | tf_op jit(solution)/shard_map/ppermute | solution.py:293
  70.8 3.6 %collective-permute-done.1.w2 = bf16[1536,256]{1,0:T(8,128)(2,1)S(1)} collective-permute-done((bf16[1536,256]{1,0:T(8,128)(2,1)S(1)}, bf16[1536,256]{1,0:T(8,128)(2,1)S(1)}, u32[]{:S(2)}, u32[]{:S(2)}) %collective-permute-start.1) | collective-permute-done | bytes 786464 | tf_op jit(solution)/shard_map/ppermute | solution.py:293
  75.3 7.4 %collective-permute-done.2.w3 = bf16[1536,256]{1,0:T(8,128)(2,1)S(1)} collective-permute-done((bf16[1536,256]{1,0:T(8,128)(2,1)S(1)}, bf16[1536,256]{1,0:T(8,128)(2,1)S(1)}, u32[]{:S(2)}, u32[]{:S(2)}) %collective-permute-start.2) | collective-permute-done | bytes 786464 | tf_op jit(solution)/shard_map/ppermute | solution.py:293
  85.9 2.8 %shard_map.134 = f32[4,776,256]{2,1,0:T(8,128)S(1)} custom-call(s32[3]{0:T(128)S(1)} %pad_add_fusion.at, bf16[4,768,256]{2,1,0:T(8,128)(2,1)S(1)} %all-to-all-done.2.tokens, bf16[1536,256]{1,0:T(8,128)(2,1)S(1)} %get-tuple-element.18.w0, bf16[1536,256]{1,0:T(8,128)(2,1)S(1)} %collective-permute-done.w1, bf16[1536,256]{1,0:T(8,128)(2,1)S(1)} %copy-done.1, ...), custom_call_target="tpu_custom_call" | custom-call | flops 1677721600 | tf_op jit(solution)/shard_map/pallas_call | solution.py:274
  89.0 16.6 %all_to_all.41 = f16[4,776,256]{2,1,0:T(8,128)(2,1)S(1)} all-to-all(f16[4,776,256]{2,1,0:T(8,128)(2,1)S(1)} %convert_element_type.14), channel_id=1, replica_groups={{0,4,8,12},{1,5,9,13},{2,6,10,14},{3,7,11,15},{16,17,18,19},{20,21,22,2..., dimensions={0} | all-to-all | bytes 3178496 | tf_op jit(solution)/shard_map/all_to_all | solution.py:298
  107.0 4.8 %all-to-all-start.4 = ((bf16[4,768,128]{2,1,0:T(8,128)(2,1)}), bf16[4,768,128]{2,1,0:T(8,128)(2,1)S(1)}, u32[]{:S(2)}, u32[]{:S(2)}) async-start(bf16[4,768,128]{2,1,0:T(8,128)(2,1)} %shard_map.135), calls=%async_computation.4 | async-start | bytes 1572864 | tf_op jit(solution)/shard_map/all_to_all | solution.py:298
  111.8 6.5 %collective-permute-start.3 = (bf16[256,128]{1,0:T(8,128)(2,1)S(1)}, bf16[256,128]{1,0:T(8,128)(2,1)S(1)}, u32[]{:S(2)}, u32[]{:S(2)}) collective-permute-start(bf16[256,128]{1,0:T(8,128)(2,1)S(1)} %shard_map.132), channel_id=1, source_target_pairs={{0,256},{32,288},{64,320},{96,352},{128,384},{160,416},{192,448},{... | collective-permute-start | bytes 196616 | tf_op jit(solution)/shard_map/ppermute | solution.py:318
  118.3 8.4 %collective-permute-done.3 = bf16[256,128]{1,0:T(8,128)(2,1)S(1)} collective-permute-done((bf16[256,128]{1,0:T(8,128)(2,1)S(1)}, bf16[256,128]{1,0:T(8,128)(2,1)S(1)}, u32[]{:S(2)}, u32[]{:S(2)}) %collective-permute-start.3) | collective-permute-done | bytes 65568 | tf_op jit(solution)/shard_map/ppermute | solution.py:318
  127.4 5.7 %collective-permute-start.4 = (bf16[512,128]{1,0:T(8,128)(2,1)}, bf16[512,128]{1,0:T(8,128)(2,1)}, u32[]{:S(2)}, u32[]{:S(2)}) collective-permute-start(bf16[512,128]{1,0:T(8,128)(2,1)} %pad_maximum_fusion.1), channel_id=1, source_target_pairs={{0,128},{32,160},{64,192},{96,224},{128,256},{160,288},{192,320},{... | collective-permute-start | bytes 393224 | tf_op jit(solution)/shard_map/ppermute | solution.py:318
  134.2 2.7 %shard_map.136 = bf16[4,768,256]{2,1,0:T(8,128)(2,1)} custom-call(s32[3]{0:T(128)S(1)} %pad_add_fusion.at, bf16[4,768,128]{2,1,0:T(8,128)(2,1)S(1)} %all-to-all-done.4.hidden, bf16[1536,256]{1,0:T(8,128)(2,1)S(1)} %get-tuple-element.18.w0, bf16[1536,256]{1,0:T(8,128)(2,1)S(1)} %collective-permute-done.w1, bf16[1536,256]{1,0:T(8,128)(2,1)S(1)} %copy-done.2, ...), custom_call_target="tpu_custom_call" | custom-call | flops 838860800 | tf_op jit(solution)/shard_map/pallas_call | solution.py:274
  137.0 5.9 %all-to-all-start.5 = ((bf16[4,768,256]{2,1,0:T(8,128)(2,1)}), bf16[4,768,256]{2,1,0:T(8,128)(2,1)S(1)}, u32[]{:S(2)}, u32[]{:S(2)}) async-start(bf16[4,768,256]{2,1,0:T(8,128)(2,1)} %shard_map.136), calls=%async_computation.5 | async-start | bytes 3145728 | tf_op jit(solution)/shard_map/all_to_all | solution.py:298
  143.8 7.8 %collective-permute-start.5 = (bf16[1024,128]{1,0:T(8,128)(2,1)S(1)}, bf16[1024,128]{1,0:T(8,128)(2,1)S(1)}, u32[]{:S(2)}, u32[]{:S(2)}) collective-permute-start(bf16[1024,128]{1,0:T(8,128)(2,1)S(1)} %pad_maximum_fusion), channel_id=1, source_target_pairs={{0,448},{32,480},{64,0},{96,32},{128,64},{160,96},{192,128},{224,1... | collective-permute-start | bytes 786440 | tf_op jit(solution)/shard_map/ppermute | solution.py:318
  152.6 9.1 %collective-permute-done.5 = bf16[1024,128]{1,0:T(8,128)(2,1)S(1)} collective-permute-done((bf16[1024,128]{1,0:T(8,128)(2,1)S(1)}, bf16[1024,128]{1,0:T(8,128)(2,1)S(1)}, u32[]{:S(2)}, u32[]{:S(2)}) %collective-permute-start.5) | collective-permute-done | bytes 262176 | tf_op jit(solution)/shard_map/ppermute | solution.py:318
  161.7 1.9 collective-permute-start.6
  164.9 4.0 %all_to_all.42 = bf16[2,384,256]{2,1,0:T(8,128)(2,1)S(1)} all-to-all(bf16[2,384,256]{2,1,0:T(8,128)(2,1)S(1)} %shard_map.137), channel_id=1, replica_groups=mesh['z'=16,'c'=2,'y'=4,'x'=4] {'c'}, dimensions={0} | all-to-all | bytes 786432 | tf_op jit(solution)/shard_map/all_to_all | solution.py:298
  169.7 8.0 %collective-permute-done.6.b = bf16[2048,128]{1,0:T(8,128)(2,1)S(1)} collective-permute-done((bf16[2048,128]{1,0:T(8,128)(2,1)S(1)}, bf16[2048,128]{1,0:T(8,128)(2,1)S(1)}, u32[]{:S(2)}, u32[]{:S(2)}) %collective-permute-start.6) | collective-permute-done | bytes 524320 | tf_op jit(solution)/shard_map/ppermute | solution.py:318
  177.8 1.9 collective-permute-start.7
  179.7 5.4 %all-to-all-start.7 = ((bf16[16,48,256]{2,1,0:T(8,128)(2,1)}), bf16[16,48,256]{2,1,0:T(8,128)(2,1)S(1)}, u32[]{:S(2)}, u32[]{:S(2)}) async-start(bf16[16,48,256]{2,1,0:T(8,128)(2,1)} %bitcast.39), calls=%async_computation.7 | async-start | bytes 786432 | tf_op jit(solution)/shard_map/all_to_all | solution.py:298
  185.2 11.6 %shard_map.143 = bf16[256,256]{1,0:T(8,128)(2,1)} custom-call(bf16[256,128]{1,0:T(8,128)(2,1)S(1)} %shard_map.138.q0, bf16[256,128]{1,0:T(8,128)(2,1)S(1)} %shard_map.139.q1, bf16[256,128]{1,0:T(8,128)(2,1)S(1)} %shard_map.140.q2, bf16[256,128]{1,0:T(8,128)(2,1)S(1)} %shard_map.141.q3, bf16[4096,128]{1,0:T(8,128)(2,1)S(1)} %shard_map.142.own, ...), custom_call_target="tpu_custom_call" | custom-call | flops 4613734400 | tf_op jit(solution)/shard_map/pallas_call | solution.py:274
  196.8 13.7 %all-to-all-done.7 = bf16[16,48,256]{2,1,0:T(8,128)(2,1)S(1)} async-done(((bf16[16,48,256]{2,1,0:T(8,128)(2,1)}), bf16[16,48,256]{2,1,0:T(8,128)(2,1)S(1)}, u32[]{:S(2)}, u32[]{:S(2)}) %all-to-all-start.7) | async-done | bytes 393248 | tf_op jit(solution)/shard_map/all_to_all | solution.py:298
  210.5 1.3 shard_map.144
  (65 shorter events, 16.6 us)
Async XLA Ops:
  0.6 0.9 copy-start.10
  1.5 0.7 copy-start.13
  2.2 17.6 %copy-start.11 = (bf16[256,64]{0,1:T(8,128)(2,1)S(1)}, bf16[256,64]{0,1:T(8,128)(2,1)}, u32[]{:S(2)}) copy-start(bf16[256,64]{0,1:T(8,128)(2,1)} %param.13) | copy-start | bytes 98308
  2.2 17.6 %copy-start.12 = (bf16[256,64]{0,1:T(8,128)(2,1)S(1)}, bf16[256,64]{0,1:T(8,128)(2,1)}, u32[]{:S(2)}) copy-start(bf16[256,64]{0,1:T(8,128)(2,1)} %param.14) | copy-start | bytes 98308
  3.4 39.0 %all-to-all-start = ((bf16[16,48,256]{2,1,0:T(8,128)(2,1)}), bf16[16,48,256]{2,1,0:T(8,128)(2,1)S(1)}, u32[]{:S(2)}, u32[]{:S(2)}) async-start(bf16[16,48,256]{2,1,0:T(8,128)(2,1)} %bitcast.4), calls=%async_computation | async-start | bytes 786432 | tf_op jit(solution)/shard_map/all_to_all | solution.py:298
  47.8 35.9 %all-to-all-start.2 = ((bf16[4,768,256]{2,1,0:T(8,128)(2,1)}), bf16[4,768,256]{2,1,0:T(8,128)(2,1)S(1)}, u32[]{:S(2)}, u32[]{:S(2)}) async-start(bf16[4,768,256]{2,1,0:T(8,128)(2,1)} %broadcast_in_dim.8), calls=%async_computation.2 | async-start | bytes 3145728 | tf_op jit(solution)/shard_map/all_to_all | solution.py:298
  52.1 1.2 copy-start.7
  53.4 1.2 copy-start.8
  54.6 1.2 copy-start.9
  56.8 14.0 %collective-permute-start = (bf16[1536,256]{1,0:T(8,128)(2,1)S(1)}, bf16[1536,256]{1,0:T(8,128)(2,1)S(1)}, u32[]{:S(2)}, u32[]{:S(2)}) collective-permute-start(bf16[1536,256]{1,0:T(8,128)(2,1)S(1)} %get-tuple-element.19), channel_id=1, source_target_pairs={{0,4},{4,8},{8,12},{12,0},{1,5},{5,9},{9,13},{13,1},{2,6},{6,10},{... | collective-permute-start | bytes 2359304 | tf_op jit(solution)/shard_map/ppermute | solution.py:293
  58.9 15.5 %collective-permute-start.1 = (bf16[1536,256]{1,0:T(8,128)(2,1)S(1)}, bf16[1536,256]{1,0:T(8,128)(2,1)S(1)}, u32[]{:S(2)}, u32[]{:S(2)}) collective-permute-start(bf16[1536,256]{1,0:T(8,128)(2,1)S(1)} %get-tuple-element.20), channel_id=1, source_target_pairs={{0,8},{4,12},{8,0},{12,4},{1,9},{5,13},{9,1},{13,5},{2,10},{6,14},... | collective-permute-start | bytes 2359304 | tf_op jit(solution)/shard_map/ppermute | solution.py:293
  63.4 19.3 %collective-permute-start.2 = (bf16[1536,256]{1,0:T(8,128)(2,1)S(1)}, bf16[1536,256]{1,0:T(8,128)(2,1)S(1)}, u32[]{:S(2)}, u32[]{:S(2)}) collective-permute-start(bf16[1536,256]{1,0:T(8,128)(2,1)S(1)} %get-tuple-element.21), channel_id=1, source_target_pairs={{0,12},{4,0},{8,4},{12,8},{1,13},{5,1},{9,5},{13,9},{2,14},{6,2},{... | collective-permute-start | bytes 2359304 | tf_op jit(solution)/shard_map/ppermute | solution.py:293
  74.4 0.9 copy-start
  82.7 0.9 copy-start.3
  83.7 1.1 copy-start.1
  84.8 1.1 copy-start.4
  105.8 27.3 %copy-start.2 = (bf16[1536,256]{1,0:T(8,128)(2,1)S(1)}, bf16[1536,256]{1,0:T(8,128)(2,1)}, u32[]{:S(2)}) copy-start(bf16[1536,256]{1,0:T(8,128)(2,1)} %copy-done) | copy-start | bytes 2359300
  107.0 26.1 %all-to-all-start.4 = ((bf16[4,768,128]{2,1,0:T(8,128)(2,1)}), bf16[4,768,128]{2,1,0:T(8,128)(2,1)S(1)}, u32[]{:S(2)}, u32[]{:S(2)}) async-start(bf16[4,768,128]{2,1,0:T(8,128)(2,1)} %shard_map.135), calls=%async_computation.4 | async-start | bytes 1572864 | tf_op jit(solution)/shard_map/all_to_all | solution.py:298
  111.8 14.9 %collective-permute-start.3 = (bf16[256,128]{1,0:T(8,128)(2,1)S(1)}, bf16[256,128]{1,0:T(8,128)(2,1)S(1)}, u32[]{:S(2)}, u32[]{:S(2)}) collective-permute-start(bf16[256,128]{1,0:T(8,128)(2,1)S(1)} %shard_map.132), channel_id=1, source_target_pairs={{0,256},{32,288},{64,320},{96,352},{128,384},{160,416},{192,448},{... | collective-permute-start | bytes 196616 | tf_op jit(solution)/shard_map/ppermute | solution.py:318
  127.4 15.5 %collective-permute-start.4 = (bf16[512,128]{1,0:T(8,128)(2,1)}, bf16[512,128]{1,0:T(8,128)(2,1)}, u32[]{:S(2)}, u32[]{:S(2)}) collective-permute-start(bf16[512,128]{1,0:T(8,128)(2,1)} %pad_maximum_fusion.1), channel_id=1, source_target_pairs={{0,128},{32,160},{64,192},{96,224},{128,256},{160,288},{192,320},{... | collective-permute-start | bytes 393224 | tf_op jit(solution)/shard_map/ppermute | solution.py:318
  133.1 1.1 copy-start.5
  136.9 26.7 %copy-start.6 = (bf16[256,256]{1,0:T(8,128)(2,1)S(1)}, bf16[256,256]{1,0:T(8,128)(2,1)}, u32[]{:S(2)}) copy-start(bf16[256,256]{1,0:T(8,128)(2,1)} %q.7) | copy-start | bytes 393220
  137.0 27.7 %all-to-all-start.5 = ((bf16[4,768,256]{2,1,0:T(8,128)(2,1)}), bf16[4,768,256]{2,1,0:T(8,128)(2,1)S(1)}, u32[]{:S(2)}, u32[]{:S(2)}) async-start(bf16[4,768,256]{2,1,0:T(8,128)(2,1)} %shard_map.136), calls=%async_computation.5 | async-start | bytes 3145728 | tf_op jit(solution)/shard_map/all_to_all | solution.py:298
  143.8 17.9 %collective-permute-start.5 = (bf16[1024,128]{1,0:T(8,128)(2,1)S(1)}, bf16[1024,128]{1,0:T(8,128)(2,1)S(1)}, u32[]{:S(2)}, u32[]{:S(2)}) collective-permute-start(bf16[1024,128]{1,0:T(8,128)(2,1)S(1)} %pad_maximum_fusion), channel_id=1, source_target_pairs={{0,448},{32,480},{64,0},{96,32},{128,64},{160,96},{192,128},{224,1... | collective-permute-start | bytes 786440 | tf_op jit(solution)/shard_map/ppermute | solution.py:318
  161.7 16.0 %collective-permute-start.6 = (bf16[2048,128]{1,0:T(8,128)(2,1)S(1)}, bf16[2048,128]{1,0:T(8,128)(2,1)S(1)}, u32[]{:S(2)}, u32[]{:S(2)}) collective-permute-start(bf16[2048,128]{1,0:T(8,128)(2,1)S(1)} %constant_dynamic-update-slice_fusion.a), channel_id=1, source_target_pairs={{0,32},{32,64},{64,96},{96,128},{128,160},{160,192},{192,224},{224... | collective-permute-start | bytes 1572872 | tf_op jit(solution)/shard_map/ppermute | solution.py:318
  177.8 7.4 %collective-permute-start.7 = (bf16[4096,128]{1,0:T(8,128)(2,1)S(1)}, bf16[4096,128]{1,0:T(8,128)(2,1)S(1)}, u32[]{:S(2)}, u32[]{:S(2)}) collective-permute-start(bf16[4096,128]{1,0:T(8,128)(2,1)S(1)} %shard_map.142.own), channel_id=1, source_target_pairs={{0,16},{16,0},{1,17},{17,1},{2,18},{18,2},{3,19},{19,3},{4,20},{20... | collective-permute-start | bytes 3145736 | tf_op jit(solution)/shard_map/ppermute | solution.py:380
  179.7 30.8 %all-to-all-start.7 = ((bf16[16,48,256]{2,1,0:T(8,128)(2,1)}), bf16[16,48,256]{2,1,0:T(8,128)(2,1)S(1)}, u32[]{:S(2)}, u32[]{:S(2)}) async-start(bf16[16,48,256]{2,1,0:T(8,128)(2,1)} %bitcast.39), calls=%async_computation.7 | async-start | bytes 786432 | tf_op jit(solution)/shard_map/all_to_all | solution.py:298
  185.1 25.4 %copy-start.14 = (s32[256,2]{0,1:T(2,128)S(1)}, s32[256,2]{0,1:T(2,128)}, u32[]{:S(2)}) copy-start(s32[256,2]{0,1:T(2,128)} %param.18) | copy-start | bytes 6148
  185.2 25.4 %copy-start.15 = (f32[256,2]{0,1:T(2,128)S(1)}, f32[256,2]{0,1:T(2,128)}, u32[]{:S(2)}) copy-start(f32[256,2]{0,1:T(2,128)} %param.20) | copy-start | bytes 6148
  185.2 25.4 %copy-start.16 = (f32[256]{0:T(256)S(1)}, f32[256]{0:T(256)}, u32[]{:S(2)}) copy-start(f32[256]{0:T(256)} %param.19) | copy-start | bytes 3076
